TPU v7x, 32 devices: a whole 2x2x4 slice. The times are simulated.
32 devices in a mesh: sp: 16 (over z, y, x), tp: 2 (over core).
Axes of the slice: x: 2, y: 2, z: 4, core: 2. Of those that a mesh axis runs over, the one named last changes fastest.
Arguments:
- residual_signal: bfloat16 [4096, 2048], P('sp'), may hold values from -6 to 6
- reading_probe_preactivations: bfloat16 [4096, 1024], P('sp', 'tp'), may hold values from -6 to 6
- keep_switch_preactivations: bfloat16 [4096, 1024], P('sp', 'tp'), may hold values from -5.5 to 5.5
- written_entries: bfloat16 [4096, 1024], P('sp', 'tp'), may hold values from -6 to 6
- emission_switch_preactivations: bfloat16 [4096, 1024], P('sp', 'tp'), may hold values from -6 to 6
- additional_shrink_amount: float32 [4096, 1024], P('sp', 'tp'), may hold values from -0.7 to 0
- complement_of_floor: float32 [1024], P('tp'), may hold values from 2.4414063e-05 to 0.1
- per_group_rescaler: float32 [128], replicated, may hold values from 0.1 to 1.9
- emission_linear_map: bfloat16 [1024, 2048], P('tp'), may hold values from -0.1875 to 0.1875
- channel_layer_rescaler: float32 [2048], replicated, may hold values from 0.1 to 1.9
- expanding_linear_map: bfloat16 [2048, 8192], P('sp', 'tp'), may hold values from -0.125 to 0.125
- contracting_linear_map: bfloat16 [2048, 8192], P('sp', 'tp'), may hold values from -0.0625 to 0.0625
Outputs:
- layer_out: bfloat16 [4096, 2048], P('sp')
All inputs are finite; a program needn't handle non-finite values.
Results may differ from a plain program's by a relative error of at most 0.006.
Values may be sent and summed in bfloat16 or wider, within the bound.
A program may use at most 128 MiB of HBM per device.

v0:
```python
import jax
import jax.numpy as jnp
from jax import lax
from jax.sharding import PartitionSpec as P

HEAD = 128
BLOCK = 64


norm_eps = 1e-06
HIGH_ACCURACY = lax.Precision.HIGHEST


def prefix(shard, axis, combine, identity):
    peers, index = (lax.axis_size(axis), lax.axis_index(axis))
    everything = jax.tree.map(lambda part: lax.all_gather(part, axis), shard)
    start = jax.tree.map(
        lambda part, zero: jnp.broadcast_to(jnp.asarray(zero, part.dtype), part.shape),
        shard,
        identity,
    )

    def turn(k, before):
        reached = k < index
        new = combine(before, jax.tree.map(lambda part: part[k], everything))
        return jax.tree.map(lambda a, b: jnp.where(reached, a, b), new, before)

    return lax.fori_loop(0, peers, turn, start)


def block_step(state_matrix, inputs):
    query_block_rows, key_blk, logs_blk, value_block_rows = inputs
    cumulative_decay = jnp.cumsum(logs_blk, axis=1)
    carried_state = jnp.einsum(
        "rlb,rbz->rlz",
        query_block_rows * jnp.exp(cumulative_decay),
        state_matrix,
        precision=HIGH_ACCURACY,
    )
    spread = cumulative_decay[:, :, None, :] - cumulative_decay[:, None, :, :]
    places = jnp.arange(BLOCK)
    lower = places[:, None] >= places[None, :]
    decay = jnp.exp(jnp.where(lower[None, :, :, None], spread, -jnp.inf))
    scores = jnp.einsum(
        "htk,hsk,htsk->hts", query_block_rows, key_blk, decay, precision=HIGH_ACCURACY
    )
    result = carried_state + jnp.einsum(
        "hts,hsv->htv", scores, value_block_rows, precision=HIGH_ACCURACY
    )
    final_state = cumulative_decay[:, -1:, :]
    decayed_key_rows = key_blk * jnp.exp(final_state - cumulative_decay)
    state_matrix = jnp.exp(final_state[:, 0, :])[..., None] * state_matrix + jnp.einsum(
        "aux,auf->axf", decayed_key_rows, value_block_rows, precision=HIGH_ACCURACY
    )
    return (state_matrix, result)


def combine_carry(earlier, later):
    return (earlier[0] * later[0], later[0][..., None] * earlier[1] + later[1])


def body(
    residual_signal,
    reading_probe_preactivations,
    keep_switch_preactivations,
    written_entries,
    emission_switch_preactivations,
    additional_shrink_amount,
    complement_of_floor,
    per_group_rescaler,
    emission_linear_map,
    channel_layer_rescaler,
    expanding_linear_map,
    contracting_linear_map,
):
    positions = reading_probe_preactivations.shape[0]
    channels = reading_probe_preactivations.shape[1]
    local_heads = channels // HEAD
    count = positions // BLOCK
    query_act = jax.nn.silu(reading_probe_preactivations.astype(jnp.float32))
    logarithmic_keep_fraction = (
        jnp.logaddexp(
            jnp.log1p(-complement_of_floor),
            jnp.log(complement_of_floor)
            + jax.nn.log_sigmoid(keep_switch_preactivations.astype(jnp.float32)),
        )
        + additional_shrink_amount
    )
    key_part = -jnp.expm1(logarithmic_keep_fraction)
    value_part = written_entries.astype(jnp.float32)

    def to_blocks(values):
        return values.reshape(count, BLOCK, local_heads, HEAD).transpose(0, 2, 1, 3)

    start = jnp.zeros((local_heads, HEAD, HEAD), jnp.float32)
    state_end, outputs = lax.scan(
        block_step,
        start,
        (
            to_blocks(query_act),
            to_blocks(key_part),
            to_blocks(logarithmic_keep_fraction),
            to_blocks(value_part),
        ),
    )
    within_block_output = outputs.transpose(0, 2, 1, 3).reshape(positions, local_heads, HEAD)
    running = jnp.cumsum(logarithmic_keep_fraction, axis=0)
    decay_total = jnp.exp(running[-1]).reshape(local_heads, HEAD)
    identity = (
        jnp.ones((local_heads, HEAD), jnp.float32),
        jnp.zeros((local_heads, HEAD, HEAD), jnp.float32),
    )
    prior_state = prefix((decay_total, state_end), "sp", combine_carry, identity)
    weighted_scores = (query_act * jnp.exp(running)).reshape(positions, local_heads, HEAD)
    recurrent_output = within_block_output + jnp.einsum(
        "pnm,nmx->pnx", weighted_scores, prior_state[1], precision=HIGH_ACCURACY
    )
    scaled = (
        recurrent_output
        * lax.rsqrt(
            jnp.mean(recurrent_output * recurrent_output, axis=-1, keepdims=True) + norm_eps
        )
        * per_group_rescaler
    )
    gated = scaled * jax.nn.silu(emission_switch_preactivations.astype(jnp.float32)).reshape(
        positions, local_heads, HEAD
    )
    mixed_heads = gated.reshape(positions, channels).astype(jnp.bfloat16)
    all_heads = lax.all_gather(mixed_heads, "tp", axis=1, tiled=True)
    full_out = lax.all_gather(emission_linear_map, "tp", axis=0, tiled=True)
    projected = jnp.dot(all_heads, full_out, preferred_element_type=jnp.float32)
    after_mix = residual_signal.astype(jnp.float32) + projected
    normed = (
        after_mix
        * lax.rsqrt(jnp.mean(after_mix * after_mix, axis=-1, keepdims=True) + norm_eps)
        * channel_layer_rescaler
    ).astype(jnp.bfloat16)
    up_whole, down_whole = (
        lax.all_gather(expanding_linear_map, "sp", axis=0, tiled=True),
        lax.all_gather(contracting_linear_map, "sp", axis=0, tiled=True),
    )
    upward = jnp.dot(normed, up_whole, preferred_element_type=jnp.float32)
    hidden = jnp.square(jax.nn.relu(upward)).astype(jnp.bfloat16)
    share = positions // lax.axis_size("tp")
    downward = lax.psum_scatter(
        lax.dot_general(
            hidden, down_whole, (((1,), (1,)), ((), ())), preferred_element_type=jnp.float32
        ),
        "tp",
        scatter_dimension=0,
        tiled=True,
    )
    own_start = lax.axis_index("tp") * share
    own_mix = lax.dynamic_slice_in_dim(after_mix, own_start, share, 0)
    finished = (own_mix + downward).astype(jnp.bfloat16)
    return lax.all_gather(finished, "tp", axis=0, tiled=True)


def solution(mesh):
    return jax.shard_map(
        body,
        mesh=mesh,
        in_specs=(
            P("sp", None),
            P("sp", "tp"),
            P("sp", "tp"),
            P("sp", "tp"),
            P("sp", "tp"),
            P("sp", "tp"),
            P("tp"),
            P(),
            P("tp", None),
            P(),
            P("sp", "tp"),
            P("sp", "tp"),
        ),
        out_specs=P("sp", None),
        check_vma=False,
    )
```

profile of v0, /device:TPU:9, one launch (start us, length us, event | category | flops | bytes accessed | tf_op | source)
XLA Modules:
  0.0 582.2 jit_solution(3244793346787176936)
XLA Ops:
  7.3 1.9 exponential-minus-one_negate_fusion
  11.7 45.1 %while.27 = (s32[]{:T(128)}, f32[4,128,128]{2,1,0:T(8,128)S(1)}, f32[4,4,64,128]{3,2,0,1:T(8,128)}, f32[4,4,64,128]{3,1,2,0:T(4,128)S(1)}, f32[4,4,64,128]{3,1,2...) while((s32[]{:T(128)}, f32[4,128,128]{2,1,0:T(8,128)S(1)}, ...), condition=%wide.region_2.3_spmd.clone, body=%wide.region_0.2_spmd.clone.sunk | while | flops 138760192 | bytes 21385852 | solution.py:96
  12.1 1.5 select_exponential_fusion.2
  13.6 7.3 %fusion.48 = f32[4,64,64]{1,2,0:T(8,128)S(1)} fusion(f32[4,64,64,128]{3,2,1,0:T(8,128)S(1)} %select_exponential_fusion.2, f32[4,128,64]{1,2,0:T(8,128)S(1)} %bitcast.106, f32[4,128,64]{1,2,0:T(8,128)S(1)} %bitcast.107), kind=kLoop, calls=%fused_computation.4.clone.1 | loop fusion | flops 6275072 | bytes 8716288 | tf_op jit(solution)/shard_map/while/body/eval_jaxpr/htk,hsk,htsk->hts/dot_general | solution.py:44
  23.3 1.5 select_exponential_fusion.2
  24.9 7.3 %fusion.48 = f32[4,64,64]{1,2,0:T(8,128)S(1)} fusion(f32[4,64,64,128]{3,2,1,0:T(8,128)S(1)} %select_exponential_fusion.2, f32[4,128,64]{1,2,0:T(8,128)S(1)} %bitcast.106, f32[4,128,64]{1,2,0:T(8,128)S(1)} %bitcast.107), kind=kLoop, calls=%fused_computation.4.clone.1 | loop fusion | flops 6275072 | bytes 8716288 | tf_op jit(solution)/shard_map/while/body/eval_jaxpr/htk,hsk,htsk->hts/dot_general | solution.py:44
  34.5 1.5 select_exponential_fusion.2
  36.1 7.3 %fusion.48 = f32[4,64,64]{1,2,0:T(8,128)S(1)} fusion(f32[4,64,64,128]{3,2,1,0:T(8,128)S(1)} %select_exponential_fusion.2, f32[4,128,64]{1,2,0:T(8,128)S(1)} %bitcast.106, f32[4,128,64]{1,2,0:T(8,128)S(1)} %bitcast.107), kind=kLoop, calls=%fused_computation.4.clone.1 | loop fusion | flops 6275072 | bytes 8716288 | tf_op jit(solution)/shard_map/while/body/eval_jaxpr/htk,hsk,htsk->hts/dot_general | solution.py:44
  45.8 1.5 select_exponential_fusion.2
  47.4 7.3 %fusion.48 = f32[4,64,64]{1,2,0:T(8,128)S(1)} fusion(f32[4,64,64,128]{3,2,1,0:T(8,128)S(1)} %select_exponential_fusion.2, f32[4,128,64]{1,2,0:T(8,128)S(1)} %bitcast.106, f32[4,128,64]{1,2,0:T(8,128)S(1)} %bitcast.107), kind=kLoop, calls=%fused_computation.4.clone.1 | loop fusion | flops 6275072 | bytes 8716288 | tf_op jit(solution)/shard_map/while/body/eval_jaxpr/htk,hsk,htsk->hts/dot_general | solution.py:44
  60.3 27.7 %all_gather.24 = f32[16,4,128]{2,1,0:T(4,128)S(1)} all-gather(f32[1,4,128]{2,1,0:T(4,128)S(1)} %bitcast.124), channel_id=1, replica_groups=mesh['sp'=16,'tp'=2] {'sp'}, dimensions={0}, use_global_device_ids=true | all-gather | bytes 34816 | tf_op jit(solution)/shard_map/all_gather | solution.py:16
  88.0 45.3 %all-gather.15.cloned.1.call-done = f32[64,128,128]{2,1,0:T(8,128)} async-done(((f32[4,128,128]{2,1,0:T(8,128)}), f32[64,128,128]{2,1,0:T(8,128)}) %all-gather.15.cloned.1.call-update) | async-done | bytes 4194320 | tf_op jit(solution)/shard_map/all_gather | solution.py:16
  133.3 19.3 %while.28 = (s32[]{:T(128)}, f32[4,128,128]{2,1,0:T(8,128)S(1)}, s32[]{:T(128)}, f32[16,4,128]{2,1,0:T(4,128)S(1)}, f32[16,4,128,128]{3,2,1,0:T(8,128)}, /*index=5*/s32[]{:T(128)}, s32[]{:T(128)}) while((s32[]{:T(128)}, f32[4,128,128]{2,1,0:T(8,128)S(1)}, s32[]{:T(128)}, f32[16,4,128]{2,1,0:T(4,128)S(1)}, ...), condition=%wide.region_6.7_spmd.clone, body=%wide.region_5.6_spmd.clone.sunk | while | flops 262148 | bytes 792681 | solution.py:28
  144.1 1.2 fusion.51
  145.4 1.2 fusion.51
  153.4 3.9 all_gather.27
  157.3 3.9 multiply_reduce_fusion
  161.1 179.6 %all-gather.11.cloned.1.call-done = bf16[2048,4096]{1,0:T(8,128)(2,1)} async-done(((bf16[128,4096]{1,0:T(8,128)(2,1)}), bf16[2048,4096]{1,0:T(8,128)(2,1)}) %all-gather.11.cloned.1.call-update) | async-done | bytes 16777232 | tf_op jit(solution)/shard_map/all_gather | solution.py:140
  340.7 191.8 %all-gather.9.cloned.1.call-done = bf16[2048,4096]{1,0:T(8,128)(2,1)} async-done(((bf16[128,4096]{1,0:T(8,128)(2,1)}), bf16[2048,4096]{1,0:T(8,128)(2,1)}) %all-gather.9.cloned.1.call-update) | async-done | bytes 16777232 | tf_op jit(solution)/shard_map/all_gather | solution.py:139
  532.6 16.4 %fusion.20 = f32[256,2048]{1,0:T(8,128)} fusion(bf16[2048,4096]{1,0:T(8,128)(2,1)} %all-gather.11.cloned.1.call-done, bf16[2048,4096]{1,0:T(8,128)(2,1)} %all-gather.9.cloned.1.call-done, f32[256,2048]{1,0:T(8,128)S(1)} %get-tuple-element.240, f32[2048]{0:T(1024)S(1)} %copy-done.7, f32[256]{0:T(256)S(1)} %add_rsqrt_fusion.1), kind=kOutput, calls=%fused_computation.44 | convolution fusion | flops 8594653184 | bytes 37757952 | tf_op jit(solution)/shard_map/dot_general | solution.py:146
  549.1 11.3 %reduce-scatter.2.cloned.1.call-done = f32[128,2048]{1,0:T(8,128)} async-done(((f32[256,2048]{1,0:T(8,128)}), f32[128,2048]{1,0:T(8,128)}) %reduce-scatter.2.cloned.1.call-update) | async-done | bytes 1048592 | tf_op jit(solution)/shard_map/reduce_scatter | solution.py:145
  560.4 2.1 add_convert_fusion
  562.5 10.5 %all-gather.13.cloned.1.call-done = bf16[256,2048]{1,0:T(8,128)(2,1)} async-done(((bf16[128,2048]{1,0:T(8,128)(2,1)}), bf16[256,2048]{1,0:T(8,128)(2,1)}) %all-gather.13.cloned.1.call-update) | async-done | bytes 1048592 | tf_op jit(solution)/shard_map/all_gather | solution.py:156
  573.0 2.3 copy.135
  (131 shorter events, 32.9 us)
Async XLA Ops:
  6.5 3.5 copy-start.3
  6.5 126.7 %all-gather.15.cloned.1.call-start = ((), (), s32[]{:S(2)}) async-start(), calls=%async_computation.6 | async-start | bytes 4456448 | tf_op jit(solution)/shard_map/all_gather | solution.py:16
  9.2 2.3 copy-start.4
  56.8 0.7 copy-start
  56.8 2.9 copy-start.2
  56.8 3.1 copy-start.5
  57.5 99.7 %all-gather.7.cloned.1.call-start = ((), (), s32[]{:S(2)}) async-start(), calls=%async_computation.1 | async-start | bytes 6291456 | tf_op jit(solution)/shard_map/all_gather | solution.py:130
  58.3 282.4 %all-gather.11.cloned.1.call-start = ((), (), s32[]{:S(2)}) async-start(), calls=%async_computation.3 | async-start | bytes 17825792 | tf_op jit(solution)/shard_map/all_gather | solution.py:140
  59.0 93.6 %copy-start.1 = (f32[32,4,8,128]{3,2,1,0:T(8,128)S(1)}, f32[32,4,8,128]{3,2,1,0:T(8,128)}, u32[]{:S(2)}) copy-start(f32[32,4,8,128]{3,2,1,0:T(8,128)} %get-tuple-element.233) | copy-start | bytes 1572868
  59.0 473.5 %all-gather.9.cloned.1.call-start = ((), (), s32[]{:S(2)}) async-start(), calls=%async_computation.2 | async-start | bytes 17825792 | tf_op jit(solution)/shard_map/all_gather | solution.py:139
  59.6 500.8 %reduce-scatter.2.cloned.1.call-start = ((), (), s32[]{:S(2)}) async-start(), calls=%async_computation.4 | async-start | bytes 3145728 | tf_op jit(solution)/shard_map/reduce_scatter | solution.py:145
  59.9 93.4 %copy-start.6 = (f32[128]{0:T(128)S(1)}, f32[128]{0:T(128)}, u32[]{:S(2)}) copy-start(f32[128]{0:T(128)} %param.23) | copy-start | bytes 1540
  157.3 375.3 %copy-start.7 = (f32[2048]{0:T(1024)S(1)}, f32[2048]{0:T(1024)}, u32[]{:S(2)}) copy-start(f32[2048]{0:T(1024)} %param.25) | copy-start | bytes 24580
  549.0 24.0 %all-gather.13.cloned.1.call-start = ((), (), s32[]{:S(2)}) async-start(), calls=%async_computation.5 | async-start | bytes 1572864 | tf_op jit(solution)/shard_map/all_gather | solution.py:156
Sparse Core Ops, SparseCore 0:
  57.7 75.5 all-gather.14
  134.8 14.1 all-gather.6
  151.8 188.8 all-gather.10
  343.3 189.1 all-gather.8
  549.1 11.2 reduce-scatter.1
  562.6 10.3 all-gather.12
where the time goes:
time: 584 us; the launch traced here: 582 us
  waiting for transfers between devices  440 us (75%)
  other arithmetic  61.1 us (10%)
  blocking collectives  31.5 us (5%)
  matrix products  29.3 us (5%)
  between operations  13.7 us (2%)
    all_gather x1, waiting for transfers between devices, body(): lax.all_gather(expanding_linear_map, 'sp', axis=0, tiled=True)  192 us
    all_gather x1, waiting for transfers between devices, body(): lax.all_gather(contracting_linear_map, 'sp', axis=0, tiled=True)  180 us
    all_gather x1, waiting for transfers between devices, prefix(): everything = jax.tree.map(lambda part: lax.all_gather(part, axis), shard)  45.3 us
    dot_general x4, other arithmetic, block_step(): jnp.einsum('htk,hsk,htsk->hts', query_block_rows, key_blk, decay, precisi...  29.3 us
    all_gather x1, blocking collectives, prefix(): everything = jax.tree.map(lambda part: lax.all_gather(part, axis), shard)  27.7 us
    select_n x16, other arithmetic, turn(): return jax.tree.map(lambda a, b: jnp.where(reached, a, b), new, before)  18.6 us
    dot_general x1, matrix products, body(): lax.dot_general(hidden, down_whole, (((1,), (1,)), ((), ())), preferred_e...  16.4 us
  transfers between devices with their start and end apart: 6, of which 5 were waited for; matrix products, arithmetic and copies ran while one was open for 4% of the time, Pallas kernels for 0%

commit v1 on v0

--- a/solution.py
+++ b/solution.py
@@ -57,6 +57,22 @@
 
 def combine_carry(earlier, later):
     return (earlier[0] * later[0], later[0][..., None] * earlier[1] + later[1])
+
+
+def grouping(peers):
+    line = plane = 4 if peers % 16 == 0 else 1
+    outer = peers // (line * plane)
+
+    def index(o, l, p):
+        return (o * line + l) * plane + p
+
+    lines = [
+        [index(o, l, p) for l in range(line)] for o in range(outer) for p in range(plane)
+    ]
+    planes = [
+        [index(o, l, p) for o in range(outer) for p in range(plane)] for l in range(line)
+    ]
+    return line, plane, outer, lines, planes
 
 
 def body(
@@ -126,33 +142,52 @@
         positions, local_heads, HEAD
     )
     mixed_heads = gated.reshape(positions, channels).astype(jnp.bfloat16)
-    all_heads = lax.all_gather(mixed_heads, "tp", axis=1, tiled=True)
+    tp = lax.axis_size("tp")
+    share = positions // tp
+    all_heads = lax.all_to_all(mixed_heads, "tp", split_axis=0, concat_axis=1, tiled=True)
     full_out = lax.all_gather(emission_linear_map, "tp", axis=0, tiled=True)
+    own_start = lax.axis_index("tp") * share
+    own_residual = lax.dynamic_slice_in_dim(residual_signal, own_start, share, 0)
     projected = jnp.dot(all_heads, full_out, preferred_element_type=jnp.float32)
-    after_mix = residual_signal.astype(jnp.float32) + projected
+    after_mix = own_residual.astype(jnp.float32) + projected
     normed = (
         after_mix
         * lax.rsqrt(jnp.mean(after_mix * after_mix, axis=-1, keepdims=True) + norm_eps)
         * channel_layer_rescaler
     ).astype(jnp.bfloat16)
-    up_whole, down_whole = (
-        lax.all_gather(expanding_linear_map, "sp", axis=0, tiled=True),
-        lax.all_gather(contracting_linear_map, "sp", axis=0, tiled=True),
-    )
-    upward = jnp.dot(normed, up_whole, preferred_element_type=jnp.float32)
+    line, plane, outer, lines, planes = grouping(lax.axis_size("sp"))
+    rows = expanding_linear_map.shape[0]
+    width = normed.shape[1]
+
+    def spread(weight):
+        mine = lax.all_to_all(
+            weight, "sp", split_axis=1, concat_axis=0, axis_index_groups=lines, tiled=True
+        )
+        return lax.all_gather(mine, "sp", axis=0, axis_index_groups=planes, tiled=True)
+
+    up_whole, down_whole = spread(expanding_linear_map), spread(contracting_linear_map)
+    ordered = (
+        normed.reshape(share, outer, line, plane, rows).swapaxes(2, 3).reshape(share, width)
+    )
+    tokens = lax.all_gather(ordered, "sp", axis=0, axis_index_groups=lines, tiled=True)
+    tokens = lax.all_gather(tokens, "tp", axis=0, tiled=True)
+    upward = jnp.dot(tokens, up_whole, preferred_element_type=jnp.float32)
     hidden = jnp.square(jax.nn.relu(upward)).astype(jnp.bfloat16)
-    share = positions // lax.axis_size("tp")
+    partial = lax.dot_general(
+        hidden, down_whole, (((1,), (1,)), ((), ())), preferred_element_type=jnp.float32
+    )
+    downward = lax.psum_scatter(partial, "tp", scatter_dimension=0, tiled=True)
     downward = lax.psum_scatter(
-        lax.dot_general(
-            hidden, down_whole, (((1,), (1,)), ((), ())), preferred_element_type=jnp.float32
-        ),
-        "tp",
+        downward.astype(jnp.bfloat16),
+        "sp",
         scatter_dimension=0,
+        axis_index_groups=lines,
         tiled=True,
     )
-    own_start = lax.axis_index("tp") * share
-    own_mix = lax.dynamic_slice_in_dim(after_mix, own_start, share, 0)
-    finished = (own_mix + downward).astype(jnp.bfloat16)
+    downward = (
+        downward.reshape(share, outer, plane, line, rows).swapaxes(2, 3).reshape(share, width)
+    )
+    finished = (after_mix + downward.astype(jnp.float32)).astype(jnp.bfloat16)
     return lax.all_gather(finished, "tp", axis=0, tiled=True)
 
 

time: 584 us -> 463 us (0.79)
  waiting for transfers between devices: 440 us -> 227 us
  blocking collectives: 31.5 us -> 106 us
  local copies, waits for them, and re-layouts: 4.77 us -> 16.7 us
    all_gather x2 -> x4, waiting for transfers between devices: 371 us -> 109 us  [the longest x2 92.5 us: spread(): lax.all_gather(mine, 'sp', axis=0, axis_index_groups=planes, tiled=True)]
    all_to_all x0 -> x2, blocking collectives: none -> 77.8 us  [spread(): lax.all_to_all(weight, 'sp', split_axis=1, concat_axis=0, axis_index_grou...]
    reduce_scatter x1 -> x2, waiting for transfers between devices: 11.3 us -> 60 us  [the longest x1 42.4 us: body(): lax.psum_scatter(downward.astype(jnp.bfloat16), 'sp', scatter_dimension=0...]
  transfers between devices with their start and end apart: 6 -> 10, of which waited for: 5 -> 8; matrix products, arithmetic and copies ran while one was open for 4% -> 6% of each run, Pallas kernels for 0% -> 0%
where the time goes in v1:
time: 463 us; the launch traced here: 461 us
  waiting for transfers between devices  227 us (49%)
  blocking collectives  106 us (23%)
  other arithmetic  65 us (14%)
  matrix products  27.1 us (6%)
  local copies, waits for them, and re-layouts  16.7 us (4%)
  between operations  13.5 us (3%)
  starting transfers between devices  5.56 us (1%)
    all_gather x2, waiting for transfers between devices, spread(): lax.all_gather(mine, 'sp', axis=0, axis_index_groups=planes, tiled=True)  92.5 us
    all_to_all x2, blocking collectives, spread(): lax.all_to_all(weight, 'sp', split_axis=1, concat_axis=0, axis_index_grou...  77.8 us
    all_gather x1, waiting for transfers between devices, prefix(): everything = jax.tree.map(lambda part: lax.all_gather(part, axis), shard)  44.5 us
    reduce_scatter x1, waiting for transfers between devices, body(): lax.psum_scatter(downward.astype(jnp.bfloat16), 'sp', scatter_dimension=0...  42.4 us
    dot_general x4, other arithmetic, block_step(): jnp.einsum('htk,hsk,htsk->hts', query_block_rows, key_blk, decay, precisi...  29.3 us
    all_gather x1, blocking collectives, prefix(): everything = jax.tree.map(lambda part: lax.all_gather(part, axis), shard)  28 us
    select_n x16, other arithmetic, turn(): return jax.tree.map(lambda a, b: jnp.where(reached, a, b), new, before)  18.7 us
    reduce_scatter x1, waiting for transfers between devices, body(): downward = lax.psum_scatter(partial, 'tp', scatter_dimension=0, tiled=True)  17.6 us
  transfers between devices with their start and end apart: 10, of which 8 were waited for; matrix products, arithmetic and copies ran while one was open for 6% of the time, Pallas kernels for 0%

profile of v1, /device:TPU:9, one launch (start us, length us, event | category | flops | bytes accessed | tf_op | source)
XLA Modules:
  0.0 461.2 jit_solution(309677073336630829)
XLA Ops:
  7.3 1.9 exponential-minus-one_negate_fusion
  11.7 45.1 %while.27 = (s32[]{:T(128)}, f32[4,128,128]{2,1,0:T(8,128)S(1)}, f32[4,4,64,128]{3,2,0,1:T(8,128)}, f32[4,4,64,128]{3,1,2,0:T(4,128)S(1)}, f32[4,4,64,128]{3,1,2...) while((s32[]{:T(128)}, f32[4,128,128]{2,1,0:T(8,128)S(1)}, ...), condition=%wide.region_2.3_spmd.clone, body=%wide.region_0.2_spmd.clone.sunk | while | flops 138760192 | bytes 21385852 | solution.py:112
  13.7 7.3 %fusion.45 = f32[4,64,64]{1,2,0:T(8,128)S(1)} fusion(f32[4,64,64,128]{3,2,1,0:T(8,128)S(1)} %select_exponential_fusion.2, f32[4,128,64]{1,2,0:T(8,128)S(1)} %bitcast.125, f32[4,128,64]{1,2,0:T(8,128)S(1)} %bitcast.126), kind=kLoop, calls=%fused_computation.4.clone.1 | loop fusion | flops 6275072 | bytes 8716288 | tf_op jit(solution)/shard_map/while/body/eval_jaxpr/htk,hsk,htsk->hts/dot_general | solution.py:44
  24.9 7.3 %fusion.45 = f32[4,64,64]{1,2,0:T(8,128)S(1)} fusion(f32[4,64,64,128]{3,2,1,0:T(8,128)S(1)} %select_exponential_fusion.2, f32[4,128,64]{1,2,0:T(8,128)S(1)} %bitcast.125, f32[4,128,64]{1,2,0:T(8,128)S(1)} %bitcast.126), kind=kLoop, calls=%fused_computation.4.clone.1 | loop fusion | flops 6275072 | bytes 8716288 | tf_op jit(solution)/shard_map/while/body/eval_jaxpr/htk,hsk,htsk->hts/dot_general | solution.py:44
  36.2 7.3 %fusion.45 = f32[4,64,64]{1,2,0:T(8,128)S(1)} fusion(f32[4,64,64,128]{3,2,1,0:T(8,128)S(1)} %select_exponential_fusion.2, f32[4,128,64]{1,2,0:T(8,128)S(1)} %bitcast.125, f32[4,128,64]{1,2,0:T(8,128)S(1)} %bitcast.126), kind=kLoop, calls=%fused_computation.4.clone.1 | loop fusion | flops 6275072 | bytes 8716288 | tf_op jit(solution)/shard_map/while/body/eval_jaxpr/htk,hsk,htsk->hts/dot_general | solution.py:44
  47.4 7.3 %fusion.45 = f32[4,64,64]{1,2,0:T(8,128)S(1)} fusion(f32[4,64,64,128]{3,2,1,0:T(8,128)S(1)} %select_exponential_fusion.2, f32[4,128,64]{1,2,0:T(8,128)S(1)} %bitcast.125, f32[4,128,64]{1,2,0:T(8,128)S(1)} %bitcast.126), kind=kLoop, calls=%fused_computation.4.clone.1 | loop fusion | flops 6275072 | bytes 8716288 | tf_op jit(solution)/shard_map/while/body/eval_jaxpr/htk,hsk,htsk->hts/dot_general | solution.py:44
  58.4 28.0 %all_gather.27 = f32[16,4,128]{2,1,0:T(4,128)S(1)} all-gather(f32[1,4,128]{2,1,0:T(4,128)S(1)} %bitcast.151), channel_id=1, replica_groups=mesh['sp'=16,'tp'=2] {'sp'}, dimensions={0}, use_global_device_ids=true | all-gather | bytes 34816 | tf_op jit(solution)/shard_map/all_gather | solution.py:16
  88.9 44.5 %all-gather.21.cloned.1.call-done = f32[64,128,128]{2,1,0:T(8,128)} async-done(((f32[4,128,128]{2,1,0:T(8,128)}), f32[64,128,128]{2,1,0:T(8,128)}) %all-gather.21.cloned.1.call-update) | async-done | bytes 4194320 | tf_op jit(solution)/shard_map/all_gather | solution.py:16
  133.4 19.4 %while.28 = (s32[]{:T(128)}, f32[4,128,128]{2,1,0:T(8,128)S(1)}, s32[]{:T(128)}, f32[16,4,128]{2,1,0:T(4,128)S(1)}, f32[16,4,128,128]{3,2,1,0:T(8,128)}, /*index=5*/s32[]{:T(128)}, s32[]{:T(128)}) while((s32[]{:T(128)}, f32[4,128,128]{2,1,0:T(8,128)S(1)}, s32[]{:T(128)}, f32[16,4,128]{2,1,0:T(4,128)S(1)}, ...), condition=%wide.region_6.7_spmd.clone, body=%wide.region_5.6_spmd.clone.sunk | while | flops 262148 | bytes 792681 | solution.py:28
  154.4 5.3 %all-to-all-start = ((bf16[2,128,512]{1,2,0:T(8,128)(2,1)}), bf16[2,128,512]{1,2,0:T(8,128)(2,1)S(1)}, u32[]{:S(2)}, u32[]{:S(2)}) async-start(bf16[2,128,512]{1,2,0:T(8,128)(2,1)} %copy.88), calls=%async_computation | async-start | bytes 524288 | tf_op jit(solution)/shard_map/all_to_all | solution.py:147
  160.9 3.0 multiply_reduce_fusion
  165.8 1.6 copy.90
  167.4 47.1 %all_to_all.54 = bf16[128,4,1024]{0,2,1:T(8,128)(2,1)S(1)} all-to-all(bf16[128,4,1024]{0,2,1:T(8,128)(2,1)S(1)} %bitcast.134), channel_id=1, replica_groups={{0,8,16,24},{2,10,18,26},{4,12,20,28},{6,14,22,30},{1,9,17,25},{3,11,19..., dimensions={1} | all-to-all | bytes 2097152 | tf_op jit(solution)/shard_map/all_to_all | solution.py:163
  217.5 30.7 %all_to_all.55 = bf16[128,4,1024]{0,2,1:T(8,128)(2,1)S(1)} all-to-all(bf16[128,4,1024]{0,2,1:T(8,128)(2,1)S(1)} %bitcast.135), channel_id=1, replica_groups={{0,8,16,24},{2,10,18,26},{4,12,20,28},{6,14,22,30},{1,9,17,25},{3,11,19..., dimensions={1} | all-to-all | bytes 2097152 | tf_op jit(solution)/shard_map/all_to_all | solution.py:163
  250.2 38.2 %all-gather.15.cloned.1.call-done = bf16[2048,1024]{1,0:T(8,128)(2,1)} async-done(((bf16[512,1024]{1,0:T(8,128)(2,1)}), bf16[2048,1024]{1,0:T(8,128)(2,1)}) %all-gather.15.cloned.1.call-update) | async-done | bytes 4194320 | tf_op jit(solution)/shard_map/all_gather | solution.py:166
  288.4 54.3 %all-gather.17.cloned.1.call-done = bf16[2048,1024]{1,0:T(8,128)(2,1)} async-done(((bf16[512,1024]{1,0:T(8,128)(2,1)}), bf16[2048,1024]{1,0:T(8,128)(2,1)}) %all-gather.17.cloned.1.call-update) | async-done | bytes 4194320 | tf_op jit(solution)/shard_map/all_gather | solution.py:166
  342.7 16.0 %all-gather.13.cloned.1.call-done = bf16[1024,2048]{0,1:T(8,128)(2,1)} async-done(((bf16[512,2048]{0,1:T(8,128)(2,1)}), bf16[1024,2048]{0,1:T(8,128)(2,1)}) %all-gather.13.cloned.1.call-update) | async-done | bytes 4194320 | tf_op jit(solution)/shard_map/all_gather | solution.py:173
  358.7 15.1 %fusion.16 = f32[1024,2048]{1,0:T(8,128)} fusion(bf16[2048,1024]{1,0:T(8,128)(2,1)} %all-gather.17.cloned.1.call-done, bf16[1024,2048]{0,1:T(8,128)(2,1)} %all-gather.13.cloned.1.call-done, bf16[2048,1024]{1,0:T(8,128)(2,1)} %all-gather.15.cloned.1.call-done), kind=kOutput, calls=%fused_computation.41 | convolution fusion | flops 8593080320 | bytes 20971520 | tf_op jit(solution)/shard_map/dot_general | solution.py:176
  373.8 17.6 %reduce-scatter.3.cloned.1.call-done = f32[512,2048]{1,0:T(8,128)} async-done(((f32[1024,2048]{1,0:T(8,128)}), f32[512,2048]{1,0:T(8,128)}) %reduce-scatter.3.cloned.1.call-update) | async-done | bytes 4194320 | tf_op jit(solution)/shard_map/reduce_scatter | solution.py:179
  391.5 3.8 convert_element_type.52
  395.4 42.4 %reduce-scatter.5.cloned.1.call-done = bf16[128,2048]{1,0:T(8,128)(2,1)} async-done(((bf16[512,2048]{1,0:T(8,128)(2,1)}), bf16[128,2048]{1,0:T(8,128)(2,1)}) %reduce-scatter.5.cloned.1.call-update) | async-done | bytes 524304 | tf_op jit(solution)/shard_map/reduce_scatter | solution.py:180
  437.8 1.9 reshape.121
  441.3 11.0 %all-gather.19.cloned.1.call-done = bf16[256,2048]{1,0:T(8,128)(2,1)} async-done(((bf16[128,2048]{1,0:T(8,128)(2,1)}), bf16[256,2048]{1,0:T(8,128)(2,1)}) %all-gather.19.cloned.1.call-update) | async-done | bytes 1048592 | tf_op jit(solution)/shard_map/all_gather | solution.py:191
  452.4 2.3 copy.175
  (154 shorter events, 52.6 us)
Async XLA Ops:
  6.5 3.5 copy-start.3
  6.5 126.9 %all-gather.21.cloned.1.call-start = ((), (), s32[]{:S(2)}) async-start(), calls=%async_computation.13 | async-start | bytes 4456448 | tf_op jit(solution)/shard_map/all_gather | solution.py:16
  9.2 2.3 copy-start.4
  56.8 0.7 copy-start
  57.6 95.2 %copy-start.1 = (f32[32,4,8,128]{3,2,1,0:T(8,128)S(1)}, f32[32,4,8,128]{3,2,1,0:T(8,128)}, u32[]{:S(2)}) copy-start(f32[32,4,8,128]{3,2,1,0:T(8,128)} %get-tuple-element.240) | copy-start | bytes 1572868
  57.6 102.1 %all-gather.9.cloned.1.call-start = ((), (), s32[]{:S(2)}) async-start(), calls=%async_computation.5 | async-start | bytes 6291456 | tf_op jit(solution)/shard_map/all_gather | solution.py:148
  86.3 67.1 %copy-start.6 = (f32[128]{0:T(128)S(1)}, f32[128]{0:T(128)}, u32[]{:S(2)}) copy-start(f32[128]{0:T(128)} %param.23) | copy-start | bytes 1540
  133.4 27.5 %copy-start.2 = (bf16[256,2048]{1,0:T(8,128)(2,1)S(1)}, bf16[256,2048]{1,0:T(8,128)(2,1)}, u32[]{:S(2)}) copy-start(bf16[256,2048]{1,0:T(8,128)(2,1)} %param.16) | copy-start | bytes 3145732
  153.5 10.4 %copy-start.5 = (f32[2048]{0:T(1024)S(1)}, f32[2048]{0:T(1024)}, u32[]{:S(2)}) copy-start(f32[2048]{0:T(1024)} %param.25) | copy-start | bytes 24580
  154.4 6.5 %all-to-all-start = ((bf16[2,128,512]{1,2,0:T(8,128)(2,1)}), bf16[2,128,512]{1,2,0:T(8,128)(2,1)S(1)}, u32[]{:S(2)}, u32[]{:S(2)}) async-start(bf16[2,128,512]{1,2,0:T(8,128)(2,1)} %copy.88), calls=%async_computation | async-start | bytes 524288 | tf_op jit(solution)/shard_map/all_to_all | solution.py:147
  159.7 89.9 %all-gather.11.cloned.1.call-start = ((), (), s32[]{:S(2)}) async-start(), calls=%async_computation.6 | async-start | bytes 2621440 | tf_op jit(solution)/shard_map/all_gather | solution.py:172
  165.7 122.7 %all-gather.15.cloned.1.call-start = ((), (), s32[]{:S(2)}) async-start(), calls=%async_computation.8 | async-start | bytes 5242880 | tf_op jit(solution)/shard_map/all_gather | solution.py:166
  215.8 126.9 %all-gather.17.cloned.1.call-start = ((), (), s32[]{:S(2)}) async-start(), calls=%async_computation.9 | async-start | bytes 5242880 | tf_op jit(solution)/shard_map/all_gather | solution.py:166
  249.5 109.1 %all-gather.13.cloned.1.call-start = ((), (), s32[]{:S(2)}) async-start(), calls=%async_computation.7 | async-start | bytes 6291456 | tf_op jit(solution)/shard_map/all_gather | solution.py:173
  250.1 141.4 %reduce-scatter.3.cloned.1.call-start = ((), (), s32[]{:S(2)}) async-start(), calls=%async_computation.10 | async-start | bytes 12582912 | tf_op jit(solution)/shard_map/reduce_scatter | solution.py:179
  373.8 64.0 %reduce-scatter.5.cloned.1.call-start = ((), (), s32[]{:S(2)}) async-start(), calls=%async_computation.11 | async-start | bytes 2621440 | tf_op jit(solution)/shard_map/reduce_scatter | solution.py:180
  395.3 57.0 %all-gather.19.cloned.1.call-start = ((), (), s32[]{:S(2)}) async-start(), calls=%async_computation.12 | async-start | bytes 1572864 | tf_op jit(solution)/shard_map/all_gather | solution.py:191
Sparse Core Ops, SparseCore 0:
  57.7 75.6 all-gather.20
  135.0 14.1 all-gather.8
  165.8 69.5 all-gather.10
  237.2 51.1 all-gather.14
  290.1 52.5 all-gather.16
  344.1 14.5 all-gather.12
  373.9 17.5 reduce-scatter.2
  395.5 42.2 reduce-scatter.4
  441.5 10.8 all-gather.18

commit v2 on v0

--- a/solution.py
+++ b/solution.py
@@ -1,6 +1,10 @@
+import functools
+
 import jax
 import jax.numpy as jnp
 from jax import lax
+from jax.experimental import pallas as pl
+from jax.experimental.pallas import tpu as pltpu
 from jax.sharding import PartitionSpec as P
 
 HEAD = 128
@@ -57,6 +61,293 @@
 
 def combine_carry(earlier, later):
     return (earlier[0] * later[0], later[0][..., None] * earlier[1] + later[1])
+
+
+MESH = pl.DeviceIdType.MESH
+TILE = 256
+
+
+def grouping(peers):
+    line = plane = 4 if peers % 16 == 0 else 1
+    return line, plane, peers // (line * plane)
+
+
+def mixer_kernel(
+    line,
+    plane,
+    outer,
+    tp,
+    normed_ref,
+    after_ref,
+    up_ref,
+    down_ref,
+    out_ref,
+    up_w,
+    down_w,
+    tok,
+    hid,
+    pair_send,
+    pair_recv,
+    keep,
+    line_send,
+    line_recv,
+    fin,
+    s1_send,
+    s1_recv,
+    s2_send,
+    s2_recv,
+    tok_send,
+    tok_recv,
+    tokp_send,
+    tokp_recv,
+    pair_ssem,
+    pair_rsem,
+    line_ssem,
+    line_rsem,
+    fin_ssem,
+    fin_rsem,
+    loc_sem,
+):
+    quads = outer * plane
+    share, width = normed_ref.shape
+    rows = up_ref.shape[0]
+    cols = up_w.shape[3]
+    me, t = lax.axis_index("sp"), lax.axis_index("tp")
+    p = lax.rem(me, plane)
+    l = lax.rem(me // plane, line)
+    o = me // (plane * line)
+    q = o * plane + p
+
+    def line_dev(d):
+        return ((o * line + lax.rem(l + d, line)) * plane + p, t)
+
+    def quad_dev(e):
+        qq = lax.rem(q + e, quads)
+        return ((qq // plane * line + l) * plane + lax.rem(qq, plane), t)
+
+    def pair_dev(f):
+        return (me, lax.rem(t + f, tp))
+
+    barrier = pltpu.get_barrier_semaphore()
+    peers = (
+        [line_dev(d) for d in range(1, line)]
+        + [quad_dev(e) for e in range(1, quads)]
+        + [pair_dev(f) for f in range(1, tp)]
+    )
+    for dev in peers:
+        pl.semaphore_signal(barrier, inc=1, device_id=dev, device_id_type=MESH)
+    pl.semaphore_wait(barrier, len(peers))
+
+    def remote(src, dst, ssem, rsem, dev):
+        return pltpu.make_async_remote_copy(
+            src_ref=src,
+            dst_ref=dst,
+            send_sem=ssem,
+            recv_sem=rsem,
+            device_id=dev,
+            device_id_type=MESH,
+        )
+
+    pending = []
+    mats = ((up_ref, up_w), (down_ref, down_w))
+
+    def first_stage(m):
+        src, dst = mats[m]
+        copies = []
+        for d in range(line):
+            there = lax.rem(l + d, line)
+            part = src.at[:, pl.ds(pl.multiple_of(there * cols, cols), cols)]
+            if d == 0:
+                copy = pltpu.make_async_copy(part, dst.at[q, l], loc_sem.at[m])
+            else:
+                k = m * line + d
+                copy = remote(part, dst.at[q, l], s1_send.at[k], s1_recv.at[k], line_dev(d))
+                pending.append(copy)
+            copy.start()
+            copies.append(copy)
+        return copies
+
+    def second_stage(m, copies):
+        dst = mats[m][1]
+        for d in range(line):
+            if d == 0:
+                copies[0].wait()
+            else:
+                copies[d].wait_recv()
+            origin = lax.rem(l + line - d, line)
+            for e in range(1, quads):
+                k = (m * line + d) * quads + e
+                copy = remote(
+                    dst.at[q, origin], dst.at[q, origin], s2_send.at[k], s2_recv.at[k], quad_dev(e)
+                )
+                copy.start()
+                arriving[m].append(copy)
+
+    arriving = ([], [])
+    own = pltpu.make_async_copy(normed_ref, tok.at[l, t], loc_sem.at[2])
+    own.start()
+    up_copies = first_stage(0)
+    token_copies = [own]
+    for d in range(1, line):
+        copy = remote(normed_ref, tok.at[l, t], tok_send.at[d], tok_recv.at[d], line_dev(d))
+        copy.start()
+        pending.append(copy)
+        token_copies.append(copy)
+    down_copies = first_stage(1)
+    second_stage(0, up_copies)
+    second_stage(1, down_copies)
+    pair_tokens = []
+    for d in range(line):
+        if d == 0:
+            own.wait()
+        else:
+            token_copies[d].wait_recv()
+        origin = lax.rem(l + line - d, line)
+        for f in range(1, tp):
+            k = d * tp + f
+            copy = remote(
+                tok.at[origin, t], tok.at[origin, t], tokp_send.at[k], tokp_recv.at[k], pair_dev(f)
+            )
+            copy.start()
+            pair_tokens.append(copy)
+    for copy in arriving[0]:
+        copy.wait()
+    for copy in pair_tokens:
+        copy.wait()
+
+    tile = min(TILE, cols)
+    for block in range(line):
+
+        @pl.loop(0, cols // tile)
+        def _(n):
+            at = pl.ds(pl.multiple_of(n * tile, tile), tile)
+            value = jnp.dot(
+                tok[block].reshape(tp * share, width),
+                up_w[:, :, :, at].reshape(width, tile),
+                preferred_element_type=jnp.float32,
+            )
+            value = jnp.maximum(value, 0.0)
+            hid[block, :, at] = (value * value).astype(jnp.bfloat16)
+
+    for copy in arriving[1]:
+        copy.wait()
+
+    def pair_copy(k, there, f):
+        other = lax.rem(t + f, tp)
+        i = k * tp + f
+        return remote(
+            pair_send.at[there, other],
+            pair_recv.at[there, f],
+            pair_ssem.at[i],
+            pair_rsem.at[i],
+            pair_dev(f),
+        )
+
+    group = width // (line * rows)
+    assert group == quads
+
+    def partial(k, there):
+        @pl.loop(0, quads)
+        def _(n):
+            at = pl.ds(pl.multiple_of(n * line * rows, line * rows), line * rows)
+            value = lax.dot_general(
+                hid[there],
+                down_w[n].reshape(line * rows, cols),
+                (((1,), (1,)), ((), ())),
+                preferred_element_type=jnp.float32,
+            ).reshape(tp, share, line * rows)
+            pair_send[there, :, :, at] = value.astype(jnp.bfloat16)
+            for c in range(tp):
+
+                @pl.when(t == c)
+                def _():
+                    keep[there, :, at] = value[c]
+
+        for f in range(1, tp):
+            pair_copy(k, there, f).start()
+
+    def combine(k, there):
+        total = keep[there]
+        for f in range(1, tp):
+            pair_copy(k, there, f).wait()
+            total = total + pair_recv[there, f].astype(jnp.float32)
+        return total
+
+    def line_copy(k, there):
+        return remote(
+            line_send.at[there], line_recv.at[l], line_ssem.at[k], line_rsem.at[k], line_dev(k)
+        )
+
+    order = list(range(1, line)) + [0]
+    for i, k in enumerate(order):
+        partial(k, lax.rem(l + k, line))
+        if i > 0:
+            before = order[i - 1]
+            there = lax.rem(l + before, line)
+            line_send[there] = combine(before, there).astype(jnp.bfloat16)
+            line_copy(before, there).start()
+    total = after_ref[...] + combine(0, l)
+    for k in range(1, line):
+        line_copy(k, lax.rem(l + k, line)).wait()
+        total = total + line_recv[lax.rem(l + line - k, line)].astype(jnp.float32)
+    fin[...] = total.astype(jnp.bfloat16)
+    out_ref[t] = fin[...]
+    last = [
+        remote(fin, out_ref.at[t], fin_ssem.at[f], fin_rsem.at[f], pair_dev(f))
+        for f in range(1, tp)
+    ]
+    for copy in last:
+        copy.start()
+    for copy in last:
+        copy.wait()
+    for copy in pending:
+        copy.wait_send()
+
+
+def mixer(normed, after_mix, up, down, line, plane, outer):
+    tp = lax.axis_size("tp")
+    quads = outer * plane
+    share, width = normed.shape
+    rows, hidden = up.shape
+    cols = hidden // line
+    bf16, f32 = jnp.bfloat16, jnp.float32
+    dma = pltpu.SemaphoreType.DMA
+    return pl.pallas_call(
+        functools.partial(mixer_kernel, line, plane, outer, tp),
+        out_shape=jax.ShapeDtypeStruct((tp, share, width), bf16),
+        in_specs=[pl.BlockSpec(memory_space=pltpu.VMEM)] * 4,
+        out_specs=pl.BlockSpec(memory_space=pltpu.VMEM),
+        scratch_shapes=[
+            pltpu.VMEM((quads, line, rows, cols), bf16),
+            pltpu.VMEM((quads, line, rows, cols), bf16),
+            pltpu.VMEM((line, tp, share, width), bf16),
+            pltpu.VMEM((line, tp * share, cols), bf16),
+            pltpu.VMEM((line, tp, share, width), bf16),
+            pltpu.VMEM((line, tp, share, width), bf16),
+            pltpu.VMEM((line, share, width), f32),
+            pltpu.VMEM((line, share, width), bf16),
+            pltpu.VMEM((line, share, width), bf16),
+            pltpu.VMEM((share, width), bf16),
+            dma((2 * line,)),
+            dma((2 * line,)),
+            dma((2 * line * quads,)),
+            dma((2 * line * quads,)),
+            dma((line,)),
+            dma((line,)),
+            dma((line * tp,)),
+            dma((line * tp,)),
+            dma((line * tp,)),
+            dma((line * tp,)),
+            dma((line,)),
+            dma((line,)),
+            dma((tp,)),
+            dma((tp,)),
+            dma((3,)),
+        ],
+        compiler_params=pltpu.CompilerParams(
+            collective_id=0, has_side_effects=True, vmem_limit_bytes=60 * 1024 * 1024
+        ),
+    )(normed, after_mix, up, down)
 
 
 def body(
@@ -126,34 +417,42 @@
         positions, local_heads, HEAD
     )
     mixed_heads = gated.reshape(positions, channels).astype(jnp.bfloat16)
-    all_heads = lax.all_gather(mixed_heads, "tp", axis=1, tiled=True)
+    tp = lax.axis_size("tp")
+    share = positions // tp
+    all_heads = lax.all_to_all(mixed_heads, "tp", split_axis=0, concat_axis=1, tiled=True)
     full_out = lax.all_gather(emission_linear_map, "tp", axis=0, tiled=True)
+    own_start = lax.axis_index("tp") * share
+    own_residual = lax.dynamic_slice_in_dim(residual_signal, own_start, share, 0)
     projected = jnp.dot(all_heads, full_out, preferred_element_type=jnp.float32)
-    after_mix = residual_signal.astype(jnp.float32) + projected
+    after_mix = own_residual.astype(jnp.float32) + projected
     normed = (
         after_mix
         * lax.rsqrt(jnp.mean(after_mix * after_mix, axis=-1, keepdims=True) + norm_eps)
         * channel_layer_rescaler
     ).astype(jnp.bfloat16)
-    up_whole, down_whole = (
-        lax.all_gather(expanding_linear_map, "sp", axis=0, tiled=True),
-        lax.all_gather(contracting_linear_map, "sp", axis=0, tiled=True),
-    )
-    upward = jnp.dot(normed, up_whole, preferred_element_type=jnp.float32)
-    hidden = jnp.square(jax.nn.relu(upward)).astype(jnp.bfloat16)
-    share = positions // lax.axis_size("tp")
-    downward = lax.psum_scatter(
-        lax.dot_general(
-            hidden, down_whole, (((1,), (1,)), ((), ())), preferred_element_type=jnp.float32
-        ),
-        "tp",
-        scatter_dimension=0,
-        tiled=True,
-    )
-    own_start = lax.axis_index("tp") * share
-    own_mix = lax.dynamic_slice_in_dim(after_mix, own_start, share, 0)
-    finished = (own_mix + downward).astype(jnp.bfloat16)
-    return lax.all_gather(finished, "tp", axis=0, tiled=True)
+    line, plane, outer = grouping(lax.axis_size("sp"))
+    rows = expanding_linear_map.shape[0]
+    width = normed.shape[1]
+
+    def ordered(values):
+        return (
+            values.reshape(share, outer, line, plane, rows).swapaxes(2, 3).reshape(share, width)
+        )
+
+    finished = mixer(
+        ordered(normed),
+        ordered(after_mix),
+        expanding_linear_map,
+        contracting_linear_map,
+        line,
+        plane,
+        outer,
+    )
+    return (
+        finished.reshape(positions, outer, plane, line, rows)
+        .swapaxes(2, 3)
+        .reshape(positions, width)
+    )
 
 
 def solution(mesh):

time: 584 us -> 356 us (0.61)
  waiting for transfers between devices: 440 us -> 46.5 us
  Pallas kernels: 0 us -> 175 us
  matrix products: 29.3 us -> 12 us
  local copies, waits for them, and re-layouts: 4.77 us -> 12.4 us
    all_gather x3 -> x0, waiting for transfers between devices: 382 us -> none  [the longest x1 192 us: body(): lax.all_gather(expanding_linear_map, 'sp', axis=0, tiled=True)]
    pallas_call x0 -> x1, Pallas kernels: none -> 175 us  [mixer(): pl.pallas_call(functools.partial(mixer_kernel, line, plane, outer, tp), o...]
    dot_general x1 -> x0, matrix products: 16.4 us -> none  [body(): lax.dot_general(hidden, down_whole, (((1,), (1,)), ((), ())), preferred_e...]
    reduce_scatter x1 -> x0, waiting for transfers between devices: 11.3 us -> none  [body(): lax.psum_scatter(lax.dot_general(hidden, down_whole, (((1,), (1,)), ((),...]
    reshape x0 -> x8, local copies, waits for them, and re-layouts: none -> 7.53 us  [the longest x6 4.14 us: ordered(): values.reshape(share, outer, line, plane, rows).swapaxes(2, 3)]
  transfers between devices with their start and end apart: 6 -> 3, of which waited for: 5 -> 2; matrix products, arithmetic and copies ran while one was open for 4% -> 6% of each run, Pallas kernels for 0% -> 0%
where the time goes in v2:
time: 356 us; the launch traced here: 355 us
  Pallas kernels  175 us (49%)
  other arithmetic  61.1 us (17%)
  waiting for transfers between devices  46.5 us (13%)
  blocking collectives  28 us (8%)
  between operations  13.7 us (4%)
  local copies, waits for them, and re-layouts  12.4 us (3%)
  matrix products  12 us (3%)
  starting transfers between devices  5.3 us (1%)
    pallas_call x1, Pallas kernels, mixer(): pl.pallas_call(functools.partial(mixer_kernel, line, plane, outer, tp), o...  175 us
    all_gather x1, waiting for transfers between devices, prefix(): everything = jax.tree.map(lambda part: lax.all_gather(part, axis), shard)  44.5 us
    dot_general x4, other arithmetic, block_step(): jnp.einsum('htk,hsk,htsk->hts', query_block_rows, key_blk, decay, precisi...  29.3 us
    all_gather x1, blocking collectives, prefix(): everything = jax.tree.map(lambda part: lax.all_gather(part, axis), shard)  28 us
    select_n x16, other arithmetic, turn(): return jax.tree.map(lambda a, b: jnp.where(reached, a, b), new, before)  18.6 us
  transfers between devices with their start and end apart: 3, of which 2 were waited for; matrix products, arithmetic and copies ran while one was open for 6% of the time, Pallas kernels for 0%

profile of v2, /device:TPU:9, one launch (start us, length us, event | category | flops | bytes accessed | tf_op | source)
XLA Modules:
  0.0 355.3 jit_solution(1548261608885864237)
XLA Ops:
  7.3 1.9 exponential-minus-one_negate_fusion
  10.0 2.0 multiply_bitcast_fusion
  12.6 45.1 %while.27 = (s32[]{:T(128)}, f32[4,128,128]{2,1,0:T(8,128)S(1)}, f32[4,4,64,128]{3,2,0,1:T(8,128)}, f32[4,4,64,128]{3,1,2,0:T(4,128)S(1)}, f32[4,4,64,128]{3,1,2...) while((s32[]{:T(128)}, f32[4,128,128]{2,1,0:T(8,128)S(1)}, ...), condition=%wide.region_2.3_spmd.clone, body=%wide.region_0.2_spmd.clone.sunk | while | flops 138760192 | bytes 21385852 | solution.py:387
  13.0 1.5 select_exponential_fusion.2
  14.6 7.3 %fusion.40 = f32[4,64,64]{1,2,0:T(8,128)S(1)} fusion(f32[4,64,64,128]{3,2,1,0:T(8,128)S(1)} %select_exponential_fusion.2, f32[4,128,64]{1,2,0:T(8,128)S(1)} %bitcast.121, f32[4,128,64]{1,2,0:T(8,128)S(1)} %bitcast.122), kind=kLoop, calls=%fused_computation.4.clone.1 | loop fusion | flops 6275072 | bytes 8716288 | tf_op jit(solution)/shard_map/while/body/eval_jaxpr/htk,hsk,htsk->hts/dot_general | solution.py:48
  24.3 1.5 select_exponential_fusion.2
  25.9 7.3 %fusion.40 = f32[4,64,64]{1,2,0:T(8,128)S(1)} fusion(f32[4,64,64,128]{3,2,1,0:T(8,128)S(1)} %select_exponential_fusion.2, f32[4,128,64]{1,2,0:T(8,128)S(1)} %bitcast.121, f32[4,128,64]{1,2,0:T(8,128)S(1)} %bitcast.122), kind=kLoop, calls=%fused_computation.4.clone.1 | loop fusion | flops 6275072 | bytes 8716288 | tf_op jit(solution)/shard_map/while/body/eval_jaxpr/htk,hsk,htsk->hts/dot_general | solution.py:48
  35.5 1.5 select_exponential_fusion.2
  37.1 7.3 %fusion.40 = f32[4,64,64]{1,2,0:T(8,128)S(1)} fusion(f32[4,64,64,128]{3,2,1,0:T(8,128)S(1)} %select_exponential_fusion.2, f32[4,128,64]{1,2,0:T(8,128)S(1)} %bitcast.121, f32[4,128,64]{1,2,0:T(8,128)S(1)} %bitcast.122), kind=kLoop, calls=%fused_computation.4.clone.1 | loop fusion | flops 6275072 | bytes 8716288 | tf_op jit(solution)/shard_map/while/body/eval_jaxpr/htk,hsk,htsk->hts/dot_general | solution.py:48
  46.7 1.5 select_exponential_fusion.2
  48.3 7.3 %fusion.40 = f32[4,64,64]{1,2,0:T(8,128)S(1)} fusion(f32[4,64,64,128]{3,2,1,0:T(8,128)S(1)} %select_exponential_fusion.2, f32[4,128,64]{1,2,0:T(8,128)S(1)} %bitcast.121, f32[4,128,64]{1,2,0:T(8,128)S(1)} %bitcast.122), kind=kLoop, calls=%fused_computation.4.clone.1 | loop fusion | flops 6275072 | bytes 8716288 | tf_op jit(solution)/shard_map/while/body/eval_jaxpr/htk,hsk,htsk->hts/dot_general | solution.py:48
  59.3 28.0 %all_gather.12 = f32[16,4,128]{2,1,0:T(4,128)S(1)} all-gather(f32[1,4,128]{2,1,0:T(4,128)S(1)} %bitcast.142), channel_id=1, replica_groups=mesh['sp'=16,'tp'=2] {'sp'}, dimensions={0}, use_global_device_ids=true | all-gather | bytes 34816 | tf_op jit(solution)/shard_map/all_gather | solution.py:20
  87.3 1.2 copy.66
  89.8 44.5 %all-gather.6.cloned.1.call-done = f32[64,128,128]{2,1,0:T(8,128)} async-done(((f32[4,128,128]{2,1,0:T(8,128)}), f32[64,128,128]{2,1,0:T(8,128)}) %all-gather.6.cloned.1.call-update) | async-done | bytes 4194320 | tf_op jit(solution)/shard_map/all_gather | solution.py:20
  134.3 19.3 %while.28 = (s32[]{:T(128)}, f32[4,128,128]{2,1,0:T(8,128)S(1)}, s32[]{:T(128)}, f32[16,4,128]{2,1,0:T(4,128)S(1)}, f32[16,4,128,128]{3,2,1,0:T(8,128)}, /*index=5*/s32[]{:T(128)}, s32[]{:T(128)}) while((s32[]{:T(128)}, f32[4,128,128]{2,1,0:T(8,128)S(1)}, s32[]{:T(128)}, f32[16,4,128]{2,1,0:T(4,128)S(1)}, ...), condition=%wide.region_6.7_spmd.clone, body=%wide.region_5.6_spmd.clone.sunk | while | flops 262148 | bytes 792681 | solution.py:32
  145.2 1.2 fusion.43
  146.4 1.2 fusion.43
  155.3 5.3 %all-to-all-start = ((bf16[2,128,512]{1,2,0:T(8,128)(2,1)}), bf16[2,128,512]{1,2,0:T(8,128)(2,1)S(1)}, u32[]{:S(2)}, u32[]{:S(2)}) async-start(bf16[2,128,512]{1,2,0:T(8,128)(2,1)} %copy.68), calls=%async_computation | async-start | bytes 524288 | tf_op jit(solution)/shard_map/all_to_all | solution.py:422
  160.5 1.3 all-to-all-done
  161.8 3.0 multiply_reduce_fusion
  165.8 1.4 reshape.120.after_ref
  169.2 175.3 %shard_map.118 = bf16[2,128,2048]{2,1,0:T(8,128)(2,1)} custom-call(bf16[128,2048]{1,0:T(8,128)(2,1)} %reshape.118.normed_ref, f32[128,2048]{1,0:T(8,128)} %reshape.120.after_ref, bf16[128,4096]{1,0:T(8,128)(2,1)} %up_ref.1, bf16[128,4096]{1,0:T(8,128)(2,1)} %down_ref.1), custom_call_target="tpu_custom_call" | custom-call | tf_op jit(solution)/shard_map/pallas_call | solution.py:315
  344.5 1.8 reshape.121
  346.9 1.6 reshape.122
  (126 shorter events, 35.5 us)
Async XLA Ops:
  6.5 5.9 %copy-start.3 = (bf16[256,512]{1,0:T(8,128)(2,1)S(1)}, bf16[256,512]{1,0:T(8,128)(2,1)}, u32[]{:S(2)}) copy-start(bf16[256,512]{1,0:T(8,128)(2,1)} %param.19) | copy-start | bytes 786436
  6.5 127.8 %all-gather.6.cloned.1.call-start = ((), (), s32[]{:S(2)}) async-start(), calls=%async_computation.2 | async-start | bytes 4456448 | tf_op jit(solution)/shard_map/all_gather | solution.py:20
  57.8 0.7 copy-start
  57.8 95.9 %copy-start.1 = (f32[32,4,8,128]{3,2,1,0:T(8,128)S(1)}, f32[32,4,8,128]{3,2,1,0:T(8,128)}, u32[]{:S(2)}) copy-start(f32[32,4,8,128]{3,2,1,0:T(8,128)} %get-tuple-element.233) | copy-start | bytes 1572868
  57.8 96.5 %copy-start.5 = (f32[128]{0:T(128)S(1)}, f32[128]{0:T(128)}, u32[]{:S(2)}) copy-start(f32[128]{0:T(128)} %param.23) | copy-start | bytes 1540
  57.8 104.0 %copy-start.2 = (bf16[256,2048]{1,0:T(8,128)(2,1)S(1)}, bf16[256,2048]{1,0:T(8,128)(2,1)}, u32[]{:S(2)}) copy-start(bf16[256,2048]{1,0:T(8,128)(2,1)} %param.16) | copy-start | bytes 3145732
  58.5 102.0 %all-gather.4.cloned.1.call-start = ((), (), s32[]{:S(2)}) async-start(), calls=%async_computation.1 | async-start | bytes 6291456 | tf_op jit(solution)/shard_map/all_gather | solution.py:423
  153.6 13.6 %copy-start.4 = (f32[2048]{0:T(1024)S(1)}, f32[2048]{0:T(1024)}, u32[]{:S(2)}) copy-start(f32[2048]{0:T(1024)} %param.25) | copy-start | bytes 24580
  155.3 6.5 %all-to-all-start = ((bf16[2,128,512]{1,2,0:T(8,128)(2,1)}), bf16[2,128,512]{1,2,0:T(8,128)(2,1)S(1)}, u32[]{:S(2)}, u32[]{:S(2)}) async-start(bf16[2,128,512]{1,2,0:T(8,128)(2,1)} %copy.68), calls=%async_computation | async-start | bytes 524288 | tf_op jit(solution)/shard_map/all_to_all | solution.py:422
Sparse Core Ops, SparseCore 0:
  58.6 75.6 all-gather.5
  135.9 14.1 all-gather.3

commit v3 on v2

--- a/solution.py
+++ b/solution.py
@@ -13,23 +13,6 @@
 
 norm_eps = 1e-06
 HIGH_ACCURACY = lax.Precision.HIGHEST
-
-
-def prefix(shard, axis, combine, identity):
-    peers, index = (lax.axis_size(axis), lax.axis_index(axis))
-    everything = jax.tree.map(lambda part: lax.all_gather(part, axis), shard)
-    start = jax.tree.map(
-        lambda part, zero: jnp.broadcast_to(jnp.asarray(zero, part.dtype), part.shape),
-        shard,
-        identity,
-    )
-
-    def turn(k, before):
-        reached = k < index
-        new = combine(before, jax.tree.map(lambda part: part[k], everything))
-        return jax.tree.map(lambda a, b: jnp.where(reached, a, b), new, before)
-
-    return lax.fori_loop(0, peers, turn, start)
 
 
 def block_step(state_matrix, inputs):
@@ -59,10 +42,6 @@
     return (state_matrix, result)
 
 
-def combine_carry(earlier, later):
-    return (earlier[0] * later[0], later[0][..., None] * earlier[1] + later[1])
-
-
 MESH = pl.DeviceIdType.MESH
 TILE = 256
 
@@ -77,11 +56,25 @@
     plane,
     outer,
     tp,
-    normed_ref,
-    after_ref,
+    payload_ref,
+    within_ref,
+    query_ref,
+    gate_ref,
+    gain_ref,
+    emission_ref,
+    residual_ref,
+    scale_ref,
     up_ref,
     down_ref,
     out_ref,
+    gathered,
+    prefixes,
+    prior,
+    mixed,
+    heads,
+    emission,
+    normed,
+    after,
     up_w,
     down_w,
     tok,
@@ -106,12 +99,24 @@
     line_rsem,
     fin_ssem,
     fin_rsem,
+    state_ssem,
+    state_rsem,
+    prior_ssem,
+    prior_rsem,
+    emis_ssem,
+    emis_rsem,
+    head_ssem,
+    head_rsem,
     loc_sem,
 ):
     quads = outer * plane
-    share, width = normed_ref.shape
+    sp = quads * line
+    share, width = normed.shape
     rows = up_ref.shape[0]
-    cols = up_w.shape[3]
+    cols = up_w.shape[2]
+    tall = prefixes.shape[1]
+    channels = emission_ref.shape[0]
+    local_heads = channels // HEAD
     me, t = lax.axis_index("sp"), lax.axis_index("tp")
     p = lax.rem(me, plane)
     l = lax.rem(me // plane, line)
@@ -125,15 +130,14 @@
         qq = lax.rem(q + e, quads)
         return ((qq // plane * line + l) * plane + lax.rem(qq, plane), t)
 
+    def seq_dev(e):
+        return (lax.rem(me + e, sp), t)
+
     def pair_dev(f):
         return (me, lax.rem(t + f, tp))
 
     barrier = pltpu.get_barrier_semaphore()
-    peers = (
-        [line_dev(d) for d in range(1, line)]
-        + [quad_dev(e) for e in range(1, quads)]
-        + [pair_dev(f) for f in range(1, tp)]
-    )
+    peers = [seq_dev(e) for e in range(1, sp)] + [pair_dev(f) for f in range(1, tp)]
     for dev in peers:
         pl.semaphore_signal(barrier, inc=1, device_id=dev, device_id_type=MESH)
     pl.semaphore_wait(barrier, len(peers))
@@ -158,10 +162,10 @@
             there = lax.rem(l + d, line)
             part = src.at[:, pl.ds(pl.multiple_of(there * cols, cols), cols)]
             if d == 0:
-                copy = pltpu.make_async_copy(part, dst.at[q, l], loc_sem.at[m])
+                copy = pltpu.make_async_copy(part, dst.at[me], loc_sem.at[m])
             else:
                 k = m * line + d
-                copy = remote(part, dst.at[q, l], s1_send.at[k], s1_recv.at[k], line_dev(d))
+                copy = remote(part, dst.at[me], s1_send.at[k], s1_recv.at[k], line_dev(d))
                 pending.append(copy)
             copy.start()
             copies.append(copy)
@@ -174,27 +178,108 @@
                 copies[0].wait()
             else:
                 copies[d].wait_recv()
-            origin = lax.rem(l + line - d, line)
+            origin = (o * line + lax.rem(l + line - d, line)) * plane + p
             for e in range(1, quads):
                 k = (m * line + d) * quads + e
                 copy = remote(
-                    dst.at[q, origin], dst.at[q, origin], s2_send.at[k], s2_recv.at[k], quad_dev(e)
+                    dst.at[origin], dst.at[origin], s2_send.at[k], s2_recv.at[k], quad_dev(e)
                 )
                 copy.start()
                 arriving[m].append(copy)
 
     arriving = ([], [])
-    own = pltpu.make_async_copy(normed_ref, tok.at[l, t], loc_sem.at[2])
+
+    state_copies = []
+    for e in range(1, sp):
+        there = lax.rem(me + e, sp)
+        copy = remote(
+            payload_ref.at[there], gathered.at[me], state_ssem.at[e], state_rsem.at[e], seq_dev(e)
+        )
+        copy.start()
+        state_copies.append(copy)
+    own = pltpu.make_async_copy(payload_ref.at[me], gathered.at[me], loc_sem.at[2])
     own.start()
+    emis_copies = [
+        pltpu.make_async_copy(emission_ref, emission.at[t], loc_sem.at[3]),
+    ]
+    for f in range(1, tp):
+        emis_copies.append(
+            remote(emission_ref, emission.at[t], emis_ssem.at[f], emis_rsem.at[f], pair_dev(f))
+        )
+    for copy in emis_copies:
+        copy.start()
     up_copies = first_stage(0)
+    own.wait()
+    for copy in state_copies:
+        copy.wait()
+    run = jnp.zeros((tall, HEAD), jnp.float32)
+    for k in range(sp):
+        prefixes[k] = run
+        run = gathered[k, tall : tall + 1, :] * run + gathered[k, :tall, :]
+    prior_copies = []
+    for e in range(1, sp):
+        there = lax.rem(me + e, sp)
+        copy = remote(
+            prefixes.at[there], prior.at[me], prior_ssem.at[e], prior_rsem.at[e], seq_dev(e)
+        )
+        copy.start()
+        prior_copies.append(copy)
+    prior[me] = prefixes[me]
+    down_copies = first_stage(1)
+    second_stage(0, up_copies)
+    for copy in prior_copies:
+        copy.wait()
+    before = prior[...].reshape(local_heads, HEAD, HEAD)
+    for h in range(local_heads):
+        lanes = slice(h * HEAD, (h + 1) * HEAD)
+        recur = within_ref[:, lanes] + lax.dot_general(
+            query_ref[:, lanes],
+            before[h],
+            (((1,), (1,)), ((), ())),
+            precision=HIGH_ACCURACY,
+            preferred_element_type=jnp.float32,
+        )
+        scaled = (
+            recur
+            * lax.rsqrt(jnp.mean(recur * recur, axis=-1, keepdims=True) + norm_eps)
+            * gain_ref[...]
+        )
+        gated = scaled * jax.nn.silu(gate_ref[:, lanes].astype(jnp.float32))
+        mixed[:, :, lanes] = gated.astype(jnp.bfloat16).reshape(tp, share, HEAD)
+    head_copies = [pltpu.make_async_copy(mixed.at[t], heads.at[t], loc_sem.at[4])]
+    for f in range(1, tp):
+        other = lax.rem(t + f, tp)
+        head_copies.append(
+            remote(mixed.at[other], heads.at[t], head_ssem.at[f], head_rsem.at[f], pair_dev(f))
+        )
+    for copy in head_copies:
+        copy.start()
+    for copy in emis_copies + head_copies:
+        copy.wait()
+    wide = min(512, width)
+
+    @pl.loop(0, width // wide)
+    def _(n):
+        at = pl.ds(pl.multiple_of(n * wide, wide), wide)
+        value = residual_ref[t, :, at].astype(jnp.float32)
+        for c in range(tp):
+            value = value + jnp.dot(
+                heads[c], emission[c, :, at], preferred_element_type=jnp.float32
+            )
+        after[:, at] = value
+
+    square = jnp.mean(after[...] * after[...], axis=-1, keepdims=True)
+    normed[...] = (after[...] * lax.rsqrt(square + norm_eps) * scale_ref[...]).astype(
+        jnp.bfloat16
+    )
+    own = pltpu.make_async_copy(normed, tok.at[l, t], loc_sem.at[5])
+    own.start()
     token_copies = [own]
     for d in range(1, line):
-        copy = remote(normed_ref, tok.at[l, t], tok_send.at[d], tok_recv.at[d], line_dev(d))
+        copy = remote(normed, tok.at[l, t], tok_send.at[d], tok_recv.at[d], line_dev(d))
         copy.start()
         pending.append(copy)
         token_copies.append(copy)
-    down_copies = first_stage(1)
-    second_stage(0, up_copies)
     second_stage(1, down_copies)
     pair_tokens = []
     for d in range(line):
@@ -223,7 +308,7 @@
             at = pl.ds(pl.multiple_of(n * tile, tile), tile)
             value = jnp.dot(
                 tok[block].reshape(tp * share, width),
-                up_w[:, :, :, at].reshape(width, tile),
+                up_w[:, :, at].reshape(width, tile),
                 preferred_element_type=jnp.float32,
             )
             value = jnp.maximum(value, 0.0)
@@ -252,7 +337,7 @@
             at = pl.ds(pl.multiple_of(n * line * rows, line * rows), line * rows)
             value = lax.dot_general(
                 hid[there],
-                down_w[n].reshape(line * rows, cols),
+                down_w[pl.ds(n * line, line)].reshape(line * rows, cols),
                 (((1,), (1,)), ((), ())),
                 preferred_element_type=jnp.float32,
             ).reshape(tp, share, line * rows)
@@ -286,7 +371,7 @@
             there = lax.rem(l + before, line)
             line_send[there] = combine(before, there).astype(jnp.bfloat16)
             line_copy(before, there).start()
-    total = after_ref[...] + combine(0, l)
+    total = after[...] + combine(0, l)
     for k in range(1, line):
         line_copy(k, lax.rem(l + k, line)).wait()
         total = total + line_recv[lax.rem(l + line - k, line)].astype(jnp.float32)
@@ -304,22 +389,36 @@
         copy.wait_send()
 
 
-def mixer(normed, after_mix, up, down, line, plane, outer):
+def mixer(
+    payload, within, query, gate, gain, out_map, residual, scale, up, down, line, plane, outer
+):
     tp = lax.axis_size("tp")
     quads = outer * plane
-    share, width = normed.shape
+    sp = quads * line
+    positions, width = residual.shape
+    share = positions // tp
     rows, hidden = up.shape
     cols = hidden // line
+    tall = payload.shape[1] - 1
+    channels = within.shape[1]
     bf16, f32 = jnp.bfloat16, jnp.float32
     dma = pltpu.SemaphoreType.DMA
     return pl.pallas_call(
         functools.partial(mixer_kernel, line, plane, outer, tp),
         out_shape=jax.ShapeDtypeStruct((tp, share, width), bf16),
-        in_specs=[pl.BlockSpec(memory_space=pltpu.VMEM)] * 4,
+        in_specs=[pl.BlockSpec(memory_space=pltpu.VMEM)] * 10,
         out_specs=pl.BlockSpec(memory_space=pltpu.VMEM),
         scratch_shapes=[
-            pltpu.VMEM((quads, line, rows, cols), bf16),
-            pltpu.VMEM((quads, line, rows, cols), bf16),
+            pltpu.VMEM((sp, tall + 1, HEAD), f32),
+            pltpu.VMEM((sp, tall, HEAD), f32),
+            pltpu.VMEM((sp, tall, HEAD), f32),
+            pltpu.VMEM((tp, share, channels), bf16),
+            pltpu.VMEM((tp, share, channels), bf16),
+            pltpu.VMEM((tp, channels, width), bf16),
+            pltpu.VMEM((share, width), bf16),
+            pltpu.VMEM((share, width), f32),
+            pltpu.VMEM((sp, rows, cols), bf16),
+            pltpu.VMEM((sp, rows, cols), bf16),
             pltpu.VMEM((line, tp, share, width), bf16),
             pltpu.VMEM((line, tp * share, cols), bf16),
             pltpu.VMEM((line, tp, share, width), bf16),
@@ -342,12 +441,31 @@
             dma((line,)),
             dma((tp,)),
             dma((tp,)),
-            dma((3,)),
+            dma((sp,)),
+            dma((sp,)),
+            dma((sp,)),
+            dma((sp,)),
+            dma((tp,)),
+            dma((tp,)),
+            dma((tp,)),
+            dma((tp,)),
+            dma((6,)),
         ],
         compiler_params=pltpu.CompilerParams(
             collective_id=0, has_side_effects=True, vmem_limit_bytes=60 * 1024 * 1024
         ),
-    )(normed, after_mix, up, down)
+    )(
+        payload,
+        within,
+        query,
+        gate,
+        gain.reshape(1, HEAD),
+        out_map,
+        residual.reshape(tp, share, width),
+        scale.reshape(1, width),
+        up,
+        down,
+    )
 
 
 def body(
@@ -397,62 +515,27 @@
     within_block_output = outputs.transpose(0, 2, 1, 3).reshape(positions, local_heads, HEAD)
     running = jnp.cumsum(logarithmic_keep_fraction, axis=0)
     decay_total = jnp.exp(running[-1]).reshape(local_heads, HEAD)
-    identity = (
-        jnp.ones((local_heads, HEAD), jnp.float32),
-        jnp.zeros((local_heads, HEAD, HEAD), jnp.float32),
-    )
-    prior_state = prefix((decay_total, state_end), "sp", combine_carry, identity)
-    weighted_scores = (query_act * jnp.exp(running)).reshape(positions, local_heads, HEAD)
-    recurrent_output = within_block_output + jnp.einsum(
-        "pnm,nmx->pnx", weighted_scores, prior_state[1], precision=HIGH_ACCURACY
-    )
-    scaled = (
-        recurrent_output
-        * lax.rsqrt(
-            jnp.mean(recurrent_output * recurrent_output, axis=-1, keepdims=True) + norm_eps
-        )
-        * per_group_rescaler
-    )
-    gated = scaled * jax.nn.silu(emission_switch_preactivations.astype(jnp.float32)).reshape(
-        positions, local_heads, HEAD
-    )
-    mixed_heads = gated.reshape(positions, channels).astype(jnp.bfloat16)
-    tp = lax.axis_size("tp")
-    share = positions // tp
-    all_heads = lax.all_to_all(mixed_heads, "tp", split_axis=0, concat_axis=1, tiled=True)
-    full_out = lax.all_gather(emission_linear_map, "tp", axis=0, tiled=True)
-    own_start = lax.axis_index("tp") * share
-    own_residual = lax.dynamic_slice_in_dim(residual_signal, own_start, share, 0)
-    projected = jnp.dot(all_heads, full_out, preferred_element_type=jnp.float32)
-    after_mix = own_residual.astype(jnp.float32) + projected
-    normed = (
-        after_mix
-        * lax.rsqrt(jnp.mean(after_mix * after_mix, axis=-1, keepdims=True) + norm_eps)
-        * channel_layer_rescaler
-    ).astype(jnp.bfloat16)
-    line, plane, outer = grouping(lax.axis_size("sp"))
-    rows = expanding_linear_map.shape[0]
-    width = normed.shape[1]
-
-    def ordered(values):
-        return (
-            values.reshape(share, outer, line, plane, rows).swapaxes(2, 3).reshape(share, width)
-        )
-
+    sp = lax.axis_size("sp")
+    tall = local_heads * HEAD // sp
+    slices = state_end.swapaxes(1, 2).reshape(sp, tall, HEAD)
+    fading = jnp.repeat(decay_total, sp // local_heads, axis=0).reshape(sp, 1, HEAD)
+    line, plane, outer = grouping(sp)
     finished = mixer(
-        ordered(normed),
-        ordered(after_mix),
+        jnp.concatenate([slices, fading], axis=1),
+        within_block_output.reshape(positions, channels),
+        query_act * jnp.exp(running),
+        emission_switch_preactivations,
+        per_group_rescaler,
+        emission_linear_map,
+        residual_signal,
+        channel_layer_rescaler,
         expanding_linear_map,
         contracting_linear_map,
         line,
         plane,
         outer,
     )
-    return (
-        finished.reshape(positions, outer, plane, line, rows)
-        .swapaxes(2, 3)
-        .reshape(positions, width)
-    )
+    return finished.reshape(residual_signal.shape)
 
 
 def solution(mesh):

time: 356 us -> 235 us (0.66)
  waiting for transfers between devices: 46.5 us -> 0 us
  blocking collectives: 28 us -> 0 us
  other arithmetic: 61.1 us -> 41.8 us
  between operations: 13.7 us -> 0.11 us
  local copies, waits for them, and re-layouts: 12.4 us -> 6.87 us
  starting transfers between devices: 5.3 us -> 0 us
  matrix products: 12 us -> 8.31 us
    all_gather x2 -> x0, waiting for transfers between devices: 44.5 us -> none  [the longest x1 44.5 us: prefix(): everything = jax.tree.map(lambda part: lax.all_gather(part, axis), shard)]
    all_gather x1 -> x0, blocking collectives: 28 us -> none  [prefix(): everything = jax.tree.map(lambda part: lax.all_gather(part, axis), shard)]
    select_n x16 -> x0, other arithmetic: 18.6 us -> none  [turn(): return jax.tree.map(lambda a, b: jnp.where(reached, a, b), new, before)]
    reshape x9 -> x0, local copies, waits for them, and re-layouts: 8.77 us -> none  [the longest x6 4.14 us: ordered(): values.reshape(share, outer, line, plane, rows).swapaxes(2, 3)]
    all_to_all x1 -> x0, starting transfers between devices: 5.26 us -> none  [body(): lax.all_to_all(mixed_heads, 'tp', split_axis=0, concat_axis=1, tiled=True)]
    dot_general x2 -> x0, matrix products: 3.66 us -> none  [the longest x1 3.01 us: body(): projected = jnp.dot(all_heads, full_out, preferred_element_type=jnp.float32)]
  transfers between devices with their start and end apart: 3 -> 0, of which waited for: 2 -> 0; matrix products, arithmetic and copies ran while one was open for 6% -> 0% of each run, Pallas kernels for 0% -> 0%
where the time goes in v3:
time: 235 us; the launch traced here: 234 us
  Pallas kernels  177 us (75%)
  other arithmetic  41.8 us (18%)
  matrix products  8.31 us (4%)
  local copies, waits for them, and re-layouts  6.87 us (3%)
    pallas_call x1, Pallas kernels, mixer(): pl.pallas_call(functools.partial(mixer_kernel, line, plane, outer, tp), o...  177 us
    dot_general x4, other arithmetic, block_step(): jnp.einsum('htk,hsk,htsk->hts', query_block_rows, key_blk, decay, precisi...  29.3 us
    exp x4, other arithmetic, block_step(): decay = jnp.exp(jnp.where(lower[None, :, :, None], spread, -jnp.inf))  6.03 us

profile of v3, /device:TPU:9, one launch (start us, length us, event | category | flops | bytes accessed | tf_op | source)
XLA Modules:
  0.0 234.3 jit_solution(14868860584518588230)
XLA Ops:
  0.0 0.7 negate_log-plus-one_fusion
  0.7 1.9 exponential-minus-one_negate_fusion
  3.7 1.1 reshape.74
  4.8 2.0 exponential_multiply_fusion
  7.1 45.1 %while.13 = (s32[]{:T(128)}, f32[4,128,128]{2,1,0:T(8,128)S(1)}, f32[4,4,64,128]{3,2,1,0:T(8,128)}, f32[4,4,64,128]{3,1,2,0:T(4,128)S(1)}, f32[4,4,64,128]{3,1,2...) while((s32[]{:T(128)}, f32[4,128,128]{2,1,0:T(8,128)S(1)}, ...), condition=%wide.region_2.3_spmd.clone, body=%wide.region_0.2_spmd.clone.sunk | while | flops 138760192 | bytes 21124744 | solution.py:505
  7.5 1.5 select_exponential_fusion.2
  9.1 7.3 %fusion.30 = f32[4,64,64]{1,2,0:T(8,128)S(1)} fusion(f32[4,64,64,128]{3,2,1,0:T(8,128)S(1)} %select_exponential_fusion.2, f32[4,128,64]{1,2,0:T(8,128)S(1)} %dynamic-slice_bitcast_fusion.2, f32[4,128,64]{1,2,0:T(8,128)S(1)} %bitcast.87), kind=kLoop, calls=%fused_computation.1.clone.1 | loop fusion | flops 6275072 | bytes 8716288 | tf_op jit(solution)/shard_map/while/body/eval_jaxpr/htk,hsk,htsk->hts/dot_general | solution.py:31
  16.8 1.0 fusion.32
  17.8 0.7 convolution_add_fusion.3
  18.7 1.5 select_exponential_fusion.2
  20.3 7.3 %fusion.30 = f32[4,64,64]{1,2,0:T(8,128)S(1)} fusion(f32[4,64,64,128]{3,2,1,0:T(8,128)S(1)} %select_exponential_fusion.2, f32[4,128,64]{1,2,0:T(8,128)S(1)} %dynamic-slice_bitcast_fusion.2, f32[4,128,64]{1,2,0:T(8,128)S(1)} %bitcast.87), kind=kLoop, calls=%fused_computation.1.clone.1 | loop fusion | flops 6275072 | bytes 8716288 | tf_op jit(solution)/shard_map/while/body/eval_jaxpr/htk,hsk,htsk->hts/dot_general | solution.py:31
  28.0 1.0 fusion.32
  29.9 1.5 select_exponential_fusion.2
  31.5 7.3 %fusion.30 = f32[4,64,64]{1,2,0:T(8,128)S(1)} fusion(f32[4,64,64,128]{3,2,1,0:T(8,128)S(1)} %select_exponential_fusion.2, f32[4,128,64]{1,2,0:T(8,128)S(1)} %dynamic-slice_bitcast_fusion.2, f32[4,128,64]{1,2,0:T(8,128)S(1)} %bitcast.87), kind=kLoop, calls=%fused_computation.1.clone.1 | loop fusion | flops 6275072 | bytes 8716288 | tf_op jit(solution)/shard_map/while/body/eval_jaxpr/htk,hsk,htsk->hts/dot_general | solution.py:31
  39.2 1.0 fusion.32
  41.2 1.5 select_exponential_fusion.2
  42.8 7.3 %fusion.30 = f32[4,64,64]{1,2,0:T(8,128)S(1)} fusion(f32[4,64,64,128]{3,2,1,0:T(8,128)S(1)} %select_exponential_fusion.2, f32[4,128,64]{1,2,0:T(8,128)S(1)} %dynamic-slice_bitcast_fusion.2, f32[4,128,64]{1,2,0:T(8,128)S(1)} %bitcast.87), kind=kLoop, calls=%fused_computation.1.clone.1 | loop fusion | flops 6275072 | bytes 8716288 | tf_op jit(solution)/shard_map/while/body/eval_jaxpr/htk,hsk,htsk->hts/dot_general | solution.py:31
  50.5 1.0 fusion.32
  51.5 0.7 convolution_add_fusion.3
  52.3 0.8 pad_maximum_fusion.payload_ref
  53.1 1.4 copy.37
  54.5 0.8 copy.65
  55.3 176.7 %shard_map.118 = bf16[2,128,2048]{2,1,0:T(8,128)(2,1)} custom-call(f32[16,33,128]{2,1,0:T(8,128)} %pad_maximum_fusion.payload_ref, f32[256,512]{1,0:T(8,128)} %bitcast.97, f32[256,512]{1,0:T(8,128)} %get-tuple-element.101.query_ref, bf16[256,512]{1,0:T(8,128)(2,1)} %gate_ref.1, f32[1,128]{1,0:T(1,128)} %bitcast.109, bf16[512,2048]{1,0:T(8,128)(2,1)} %emission_ref.1, ...), custom_call_target="tpu_custom_call" | custom-call | tf_op jit(solution)/shard_map/pallas_call | solution.py:406
  232.0 2.3 copy.90
  (58 shorter events, 5.2 us)

commit v4 on v3

--- a/solution.py
+++ b/solution.py
@@ -15,33 +15,6 @@
 HIGH_ACCURACY = lax.Precision.HIGHEST
 
 
-def block_step(state_matrix, inputs):
-    query_block_rows, key_blk, logs_blk, value_block_rows = inputs
-    cumulative_decay = jnp.cumsum(logs_blk, axis=1)
-    carried_state = jnp.einsum(
-        "rlb,rbz->rlz",
-        query_block_rows * jnp.exp(cumulative_decay),
-        state_matrix,
-        precision=HIGH_ACCURACY,
-    )
-    spread = cumulative_decay[:, :, None, :] - cumulative_decay[:, None, :, :]
-    places = jnp.arange(BLOCK)
-    lower = places[:, None] >= places[None, :]
-    decay = jnp.exp(jnp.where(lower[None, :, :, None], spread, -jnp.inf))
-    scores = jnp.einsum(
-        "htk,hsk,htsk->hts", query_block_rows, key_blk, decay, precision=HIGH_ACCURACY
-    )
-    result = carried_state + jnp.einsum(
-        "hts,hsv->htv", scores, value_block_rows, precision=HIGH_ACCURACY
-    )
-    final_state = cumulative_decay[:, -1:, :]
-    decayed_key_rows = key_blk * jnp.exp(final_state - cumulative_decay)
-    state_matrix = jnp.exp(final_state[:, 0, :])[..., None] * state_matrix + jnp.einsum(
-        "aux,auf->axf", decayed_key_rows, value_block_rows, precision=HIGH_ACCURACY
-    )
-    return (state_matrix, result)
-
-
 MESH = pl.DeviceIdType.MESH
 TILE = 256
 
@@ -56,9 +29,10 @@
     plane,
     outer,
     tp,
-    payload_ref,
-    within_ref,
-    query_ref,
+    probe_ref,
+    logs_ref,
+    key_ref,
+    value_ref,
     gate_ref,
     gain_ref,
     emission_ref,
@@ -67,6 +41,11 @@
     up_ref,
     down_ref,
     out_ref,
+    payload_ref,
+    within_ref,
+    query_ref,
+    state,
+    base,
     gathered,
     prefixes,
     prior,
@@ -189,16 +168,6 @@
 
     arriving = ([], [])
 
-    state_copies = []
-    for e in range(1, sp):
-        there = lax.rem(me + e, sp)
-        copy = remote(
-            payload_ref.at[there], gathered.at[me], state_ssem.at[e], state_rsem.at[e], seq_dev(e)
-        )
-        copy.start()
-        state_copies.append(copy)
-    own = pltpu.make_async_copy(payload_ref.at[me], gathered.at[me], loc_sem.at[2])
-    own.start()
     emis_copies = [
         pltpu.make_async_copy(emission_ref, emission.at[t], loc_sem.at[3]),
     ]
@@ -209,6 +178,57 @@
     for copy in emis_copies:
         copy.start()
     up_copies = first_stage(0)
+    state[...] = jnp.zeros_like(state)
+    base[...] = jnp.zeros_like(base)
+    lower = lax.broadcasted_iota(jnp.int32, (BLOCK, BLOCK), 0) >= lax.broadcasted_iota(
+        jnp.int32, (BLOCK, BLOCK), 1
+    )
+
+    def exact(a, b, ca, cb):
+        return lax.dot_general(
+            a,
+            b,
+            (((ca,), (cb,)), ((), ())),
+            precision=HIGH_ACCURACY,
+            preferred_element_type=jnp.float32,
+        )
+
+    @pl.loop(0, probe_ref.shape[0] // BLOCK)
+    def _(b):
+        at = pl.ds(pl.multiple_of(b * BLOCK, BLOCK), BLOCK)
+        sums = exact(lower.astype(jnp.float32), logs_ref[at, :], 1, 0)
+        for h in range(local_heads):
+            lanes = slice(h * HEAD, (h + 1) * HEAD)
+            total = sums[:, lanes]
+            end = total[BLOCK - 1 : BLOCK, :]
+            middle = 0.5 * end
+            query = jax.nn.silu(probe_ref[at, lanes].astype(jnp.float32))
+            key = key_ref[at, lanes]
+            value = value_ref[at, lanes].astype(jnp.float32)
+            scores = exact(query * jnp.exp(total - middle), key * jnp.exp(middle - total), 1, 1)
+            scores = jnp.where(lower, scores, 0.0)
+            within_ref[at, lanes] = exact(scores, value, 1, 0) + exact(
+                query * jnp.exp(total), state[h], 1, 1
+            )
+            query_ref[at, lanes] = query * jnp.exp(base[h] + total)
+            state[h] = jnp.exp(end) * state[h] + exact(value, key * jnp.exp(end - total), 0, 0)
+            base[h] = base[h] + end
+
+    each = sp // local_heads
+    for k in range(sp):
+        h, j = divmod(k, each)
+        payload_ref[k, :tall, :] = state[h, j * tall : (j + 1) * tall, :]
+        payload_ref[k, tall : tall + 1, :] = jnp.exp(base[h])
+    state_copies = []
+    for e in range(1, sp):
+        there = lax.rem(me + e, sp)
+        copy = remote(
+            payload_ref.at[there], gathered.at[me], state_ssem.at[e], state_rsem.at[e], seq_dev(e)
+        )
+        copy.start()
+        state_copies.append(copy)
+    own = pltpu.make_async_copy(payload_ref.at[me], gathered.at[me], loc_sem.at[2])
+    own.start()
     own.wait()
     for copy in state_copies:
         copy.wait()
@@ -390,7 +410,20 @@
 
 
 def mixer(
-    payload, within, query, gate, gain, out_map, residual, scale, up, down, line, plane, outer
+    probe,
+    logs,
+    key,
+    value,
+    gate,
+    gain,
+    out_map,
+    residual,
+    scale,
+    up,
+    down,
+    line,
+    plane,
+    outer,
 ):
     tp = lax.axis_size("tp")
     quads = outer * plane
@@ -399,16 +432,22 @@
     share = positions // tp
     rows, hidden = up.shape
     cols = hidden // line
-    tall = payload.shape[1] - 1
-    channels = within.shape[1]
+    channels = probe.shape[1]
+    heads = channels // HEAD
+    tall = channels // sp
     bf16, f32 = jnp.bfloat16, jnp.float32
     dma = pltpu.SemaphoreType.DMA
     return pl.pallas_call(
         functools.partial(mixer_kernel, line, plane, outer, tp),
         out_shape=jax.ShapeDtypeStruct((tp, share, width), bf16),
-        in_specs=[pl.BlockSpec(memory_space=pltpu.VMEM)] * 10,
+        in_specs=[pl.BlockSpec(memory_space=pltpu.VMEM)] * 11,
         out_specs=pl.BlockSpec(memory_space=pltpu.VMEM),
         scratch_shapes=[
+            pltpu.VMEM((sp, tall + 1, HEAD), f32),
+            pltpu.VMEM((positions, channels), f32),
+            pltpu.VMEM((positions, channels), f32),
+            pltpu.VMEM((heads, HEAD, HEAD), f32),
+            pltpu.VMEM((heads, 1, HEAD), f32),
             pltpu.VMEM((sp, tall + 1, HEAD), f32),
             pltpu.VMEM((sp, tall, HEAD), f32),
             pltpu.VMEM((sp, tall, HEAD), f32),
@@ -455,9 +494,10 @@
             collective_id=0, has_side_effects=True, vmem_limit_bytes=60 * 1024 * 1024
         ),
     )(
-        payload,
-        within,
-        query,
+        probe,
+        logs,
+        key,
+        value,
         gate,
         gain.reshape(1, HEAD),
         out_map,
@@ -482,11 +522,6 @@
     expanding_linear_map,
     contracting_linear_map,
 ):
-    positions = reading_probe_preactivations.shape[0]
-    channels = reading_probe_preactivations.shape[1]
-    local_heads = channels // HEAD
-    count = positions // BLOCK
-    query_act = jax.nn.silu(reading_probe_preactivations.astype(jnp.float32))
     logarithmic_keep_fraction = (
         jnp.logaddexp(
             jnp.log1p(-complement_of_floor),
@@ -496,34 +531,12 @@
         + additional_shrink_amount
     )
     key_part = -jnp.expm1(logarithmic_keep_fraction)
-    value_part = written_entries.astype(jnp.float32)
-
-    def to_blocks(values):
-        return values.reshape(count, BLOCK, local_heads, HEAD).transpose(0, 2, 1, 3)
-
-    start = jnp.zeros((local_heads, HEAD, HEAD), jnp.float32)
-    state_end, outputs = lax.scan(
-        block_step,
-        start,
-        (
-            to_blocks(query_act),
-            to_blocks(key_part),
-            to_blocks(logarithmic_keep_fraction),
-            to_blocks(value_part),
-        ),
-    )
-    within_block_output = outputs.transpose(0, 2, 1, 3).reshape(positions, local_heads, HEAD)
-    running = jnp.cumsum(logarithmic_keep_fraction, axis=0)
-    decay_total = jnp.exp(running[-1]).reshape(local_heads, HEAD)
-    sp = lax.axis_size("sp")
-    tall = local_heads * HEAD // sp
-    slices = state_end.swapaxes(1, 2).reshape(sp, tall, HEAD)
-    fading = jnp.repeat(decay_total, sp // local_heads, axis=0).reshape(sp, 1, HEAD)
-    line, plane, outer = grouping(sp)
+    line, plane, outer = grouping(lax.axis_size("sp"))
     finished = mixer(
-        jnp.concatenate([slices, fading], axis=1),
-        within_block_output.reshape(positions, channels),
-        query_act * jnp.exp(running),
+        reading_probe_preactivations,
+        logarithmic_keep_fraction,
+        key_part,
+        written_entries,
         emission_switch_preactivations,
         per_group_rescaler,
         emission_linear_map,

time: 235 us -> 194 us (0.83)
  other arithmetic: 41.8 us -> 3.59 us
  Pallas kernels: 177 us -> 187 us
  matrix products: 8.31 us -> 0 us
  local copies, waits for them, and re-layouts: 6.87 us -> 2.3 us
    dot_general x4 -> x0, other arithmetic: 29.3 us -> none  [block_step(): jnp.einsum('htk,hsk,htsk->hts', query_block_rows, key_blk, decay, precisi...]
    pallas_call x1, Pallas kernels: 177 us -> 187 us  [mixer(): pl.pallas_call(functools.partial(mixer_kernel, line, plane, outer, tp), o...]
    dot_general x12 -> x0, matrix products: 8.31 us -> none  [the longest x4 4.13 us: block_step(): jnp.einsum('rlb,rbz->rlz', query_block_rows * jnp.exp(cumulative_decay),...]
    exp x4 -> x0, other arithmetic: 6.03 us -> none  [block_step(): decay = jnp.exp(jnp.where(lower[None, :, :, None], spread, -jnp.inf))]
    transpose x3 -> x0, local copies, waits for them, and re-layouts: 2.63 us -> none  [the longest x1 1.38 us: body(): outputs.transpose(0, 2, 1, 3).reshape(positions, local_heads, HEAD)]
where the time goes in v4:
time: 194 us; the launch traced here: 193 us
  Pallas kernels  187 us (96%)
  other arithmetic  3.59 us (2%)
  local copies, waits for them, and re-layouts  2.3 us (1%)
    pallas_call x1, Pallas kernels, mixer(): pl.pallas_call(functools.partial(mixer_kernel, line, plane, outer, tp), o...  187 us

profile of v4, /device:TPU:9, one launch (start us, length us, event | category | flops | bytes accessed | tf_op | source)
XLA Modules:
  0.0 193.3 jit_solution(9758369292699359418)
XLA Ops:
  0.0 0.7 negate_log-plus-one_fusion
  0.7 2.9 %exponential-minus-one_negate_fusion = (f32[256,512]{1,0:T(8,128)}, f32[256,512]{1,0:T(8,128)}) fusion(f32[256,512]{1,0:T(8,128)} %param.17, bf16[256,512]{1,0:T(8,128)(2,1)} %param.14, f32[512]{0:T(512)S(1)} %get-tuple-element.8, f32[512]{0:T(512)S(1)} %get-tuple-element.7), kind=kLoop, calls=%fused_computation.3 | loop fusion | flops 2621440 | bytes 1839104 | tf_op jit(solution)/shard_map/neg | solution.py:533
  3.6 187.4 %shard_map.118 = bf16[2,128,2048]{2,1,0:T(8,128)(2,1)} custom-call(bf16[256,512]{1,0:T(8,128)(2,1)} %probe_ref.1, f32[256,512]{1,0:T(8,128)} %get-tuple-element.6.logs_ref, f32[256,512]{1,0:T(8,128)} %get-tuple-element.5.key_ref, bf16[256,512]{1,0:T(8,128)(2,1)} %value_ref.1, bf16[256,512]{1,0:T(8,128)(2,1)} %gate_ref.1, f32[1,128]{1,0:T(1,128)} %bitcast.7, ...), custom_call_target="tpu_custom_call" | custom-call | tf_op jit(solution)/shard_map/pallas_call | solution.py:440
  191.0 2.3 %copy.14 = bf16[256,2048]{1,0:T(8,128)(2,1)} copy(bf16[256,2048]{1,0:T(8,128)(2,1)} %bitcast.4) | data formatting | bytes 2097152

commit v5 on v4

--- a/solution.py
+++ b/solution.py
@@ -301,28 +301,28 @@
         pending.append(copy)
         token_copies.append(copy)
     second_stage(1, down_copies)
-    pair_tokens = []
-    for d in range(line):
+    for copy in arriving[0]:
+        copy.wait()
+    tile = min(TILE, cols)
+
+    def receive(d):
+        origin = lax.rem(l + line - d, line)
         if d == 0:
             own.wait()
         else:
             token_copies[d].wait_recv()
-        origin = lax.rem(l + line - d, line)
+        copies = []
         for f in range(1, tp):
             k = d * tp + f
             copy = remote(
                 tok.at[origin, t], tok.at[origin, t], tokp_send.at[k], tokp_recv.at[k], pair_dev(f)
             )
             copy.start()
-            pair_tokens.append(copy)
-    for copy in arriving[0]:
-        copy.wait()
-    for copy in pair_tokens:
-        copy.wait()
-
-    tile = min(TILE, cols)
-    for block in range(line):
-
+            copies.append(copy)
+        for copy in copies:
+            copy.wait()
+
+    def expand(block):
         @pl.loop(0, cols // tile)
         def _(n):
             at = pl.ds(pl.multiple_of(n * tile, tile), tile)
@@ -333,9 +333,6 @@
             )
             value = jnp.maximum(value, 0.0)
             hid[block, :, at] = (value * value).astype(jnp.bfloat16)
-
-    for copy in arriving[1]:
-        copy.wait()
 
     def pair_copy(k, there, f):
         other = lax.rem(t + f, tp)
@@ -383,14 +380,22 @@
             line_send.at[there], line_recv.at[l], line_ssem.at[k], line_rsem.at[k], line_dev(k)
         )
 
-    order = list(range(1, line)) + [0]
-    for i, k in enumerate(order):
-        partial(k, lax.rem(l + k, line))
-        if i > 0:
-            before = order[i - 1]
-            there = lax.rem(l + before, line)
-            line_send[there] = combine(before, there).astype(jnp.bfloat16)
-            line_copy(before, there).start()
+    def send_line(k):
+        there = lax.rem(l + k, line)
+        line_send[there] = combine(k, there).astype(jnp.bfloat16)
+        line_copy(k, there).start()
+
+    for d in range(line):
+        k = (line - d) % line
+        there = lax.rem(l + k, line)
+        receive(d)
+        expand(there)
+        if d == 0:
+            for copy in arriving[1]:
+                copy.wait()
+        partial(k, there)
+        if k:
+            send_line(k)
     total = after[...] + combine(0, l)
     for k in range(1, line):
         line_copy(k, lax.rem(l + k, line)).wait()

time: 194 us -> 200 us (1.031)
  Pallas kernels: 187 us -> 192 us
    pallas_call x1, Pallas kernels: 187 us -> 192 us  [mixer(): pl.pallas_call(functools.partial(mixer_kernel, line, plane, outer, tp), o...]
where the time goes in v5:
time: 200 us; the launch traced here: 198 us
  Pallas kernels  192 us (96%)
  other arithmetic  3.59 us (2%)
  local copies, waits for them, and re-layouts  2.3 us (1%)
    pallas_call x1, Pallas kernels, mixer(): pl.pallas_call(functools.partial(mixer_kernel, line, plane, outer, tp), o...  192 us

profile of v5, /device:TPU:9, one launch (start us, length us, event | category | flops | bytes accessed | tf_op | source)
XLA Modules:
  0.0 198.1 jit_solution(5760434598182446322)
XLA Ops:
  0.0 0.7 negate_log-plus-one_fusion
  0.7 2.9 %exponential-minus-one_negate_fusion = (f32[256,512]{1,0:T(8,128)}, f32[256,512]{1,0:T(8,128)}) fusion(f32[256,512]{1,0:T(8,128)} %param.17, bf16[256,512]{1,0:T(8,128)(2,1)} %param.14, f32[512]{0:T(512)S(1)} %get-tuple-element.8, f32[512]{0:T(512)S(1)} %get-tuple-element.7), kind=kLoop, calls=%fused_computation.3 | loop fusion | flops 2621440 | bytes 1839104 | tf_op jit(solution)/shard_map/neg | solution.py:538
  3.6 192.2 %shard_map.118 = bf16[2,128,2048]{2,1,0:T(8,128)(2,1)} custom-call(bf16[256,512]{1,0:T(8,128)(2,1)} %probe_ref.1, f32[256,512]{1,0:T(8,128)} %get-tuple-element.6.logs_ref, f32[256,512]{1,0:T(8,128)} %get-tuple-element.5.key_ref, bf16[256,512]{1,0:T(8,128)(2,1)} %value_ref.1, bf16[256,512]{1,0:T(8,128)(2,1)} %gate_ref.1, f32[1,128]{1,0:T(1,128)} %bitcast.7, ...), custom_call_target="tpu_custom_call" | custom-call | tf_op jit(solution)/shard_map/pallas_call | solution.py:445
  195.8 2.3 %copy.14 = bf16[256,2048]{1,0:T(8,128)(2,1)} copy(bf16[256,2048]{1,0:T(8,128)(2,1)} %bitcast.4) | data formatting | bytes 2097152

commit v6 on v4

--- a/solution.py
+++ b/solution.py
@@ -150,9 +150,9 @@
             copies.append(copy)
         return copies
 
-    def second_stage(m, copies):
+    def second_stage(m, copies, steps):
         dst = mats[m][1]
-        for d in range(line):
+        for d in steps:
             if d == 0:
                 copies[0].wait()
             else:
@@ -178,6 +178,7 @@
     for copy in emis_copies:
         copy.start()
     up_copies = first_stage(0)
+    second_stage(0, up_copies, range(1))
     state[...] = jnp.zeros_like(state)
     base[...] = jnp.zeros_like(base)
     lower = lax.broadcasted_iota(jnp.int32, (BLOCK, BLOCK), 0) >= lax.broadcasted_iota(
@@ -229,6 +230,7 @@
         state_copies.append(copy)
     own = pltpu.make_async_copy(payload_ref.at[me], gathered.at[me], loc_sem.at[2])
     own.start()
+    second_stage(0, up_copies, range(1, line))
     own.wait()
     for copy in state_copies:
         copy.wait()
@@ -246,7 +248,7 @@
         prior_copies.append(copy)
     prior[me] = prefixes[me]
     down_copies = first_stage(1)
-    second_stage(0, up_copies)
+    second_stage(1, down_copies, range(1))
     for copy in prior_copies:
         copy.wait()
     before = prior[...].reshape(local_heads, HEAD, HEAD)
@@ -300,7 +302,7 @@
         copy.start()
         pending.append(copy)
         token_copies.append(copy)
-    second_stage(1, down_copies)
+    second_stage(1, down_copies, range(1, line))
     pair_tokens = []
     for d in range(line):
         if d == 0:

time: 194 us -> 187 us (0.964)
  Pallas kernels: 187 us -> 179 us
    pallas_call x1, Pallas kernels: 187 us -> 179 us  [mixer(): pl.pallas_call(functools.partial(mixer_kernel, line, plane, outer, tp), o...]
where the time goes in v6:
time: 187 us; the launch traced here: 185 us
  Pallas kernels  179 us (96%)
  other arithmetic  3.59 us (2%)
  local copies, waits for them, and re-layouts  2.3 us (1%)
    pallas_call x1, Pallas kernels, mixer(): pl.pallas_call(functools.partial(mixer_kernel, line, plane, outer, tp), o...  179 us

profile of v6, /device:TPU:9, one launch (start us, length us, event | category | flops | bytes accessed | tf_op | source)
XLA Modules:
  0.0 184.7 jit_solution(12052449919913539880)
XLA Ops:
  0.0 0.7 negate_log-plus-one_fusion
  0.7 2.9 %exponential-minus-one_negate_fusion = (f32[256,512]{1,0:T(8,128)}, f32[256,512]{1,0:T(8,128)}) fusion(f32[256,512]{1,0:T(8,128)} %param.17, bf16[256,512]{1,0:T(8,128)(2,1)} %param.14, f32[512]{0:T(512)S(1)} %get-tuple-element.8, f32[512]{0:T(512)S(1)} %get-tuple-element.7), kind=kLoop, calls=%fused_computation.3 | loop fusion | flops 2621440 | bytes 1839104 | tf_op jit(solution)/shard_map/neg | solution.py:535
  3.6 178.8 %shard_map.118 = bf16[2,128,2048]{2,1,0:T(8,128)(2,1)} custom-call(bf16[256,512]{1,0:T(8,128)(2,1)} %probe_ref.1, f32[256,512]{1,0:T(8,128)} %get-tuple-element.6.logs_ref, f32[256,512]{1,0:T(8,128)} %get-tuple-element.5.key_ref, bf16[256,512]{1,0:T(8,128)(2,1)} %value_ref.1, bf16[256,512]{1,0:T(8,128)(2,1)} %gate_ref.1, f32[1,128]{1,0:T(1,128)} %bitcast.7, ...), custom_call_target="tpu_custom_call" | custom-call | tf_op jit(solution)/shard_map/pallas_call | solution.py:442
  182.4 2.3 %copy.14 = bf16[256,2048]{1,0:T(8,128)(2,1)} copy(bf16[256,2048]{1,0:T(8,128)(2,1)} %bitcast.4) | data formatting | bytes 2097152
